TPU v7x, 32 devices: a whole 2x2x4 slice. The times are simulated.
32 devices in a mesh: sp: 8 (over z, x), tp: 4 (over y, core).
Axes of the slice: x: 2, y: 2, z: 4, core: 2. Of those that a mesh axis runs over, the one named last changes fastest.
Arguments:
- residual: bfloat16 [1536, 2048], P('sp', 'tp'), may hold values from -10 to 10
- queries: bfloat16 [1536, 16, 128], P('sp', 'tp'), may hold values from -6.5 to 6.5
- key_rows: bfloat16 [1536, 16, 128], P('sp', 'tp'), may hold values from -6.5 to 6.5
- value_rows: bfloat16 [1536, 16, 128], P('sp', 'tp'), may hold values from -6 to 6
- diff_scale: float32 [16], P('tp'), may hold values from 0.3 to 0.8
- head_gain: float32 [128], replicated, may hold values from 0.1 to 1.9
- out_weight: bfloat16 [2048, 2048], P(None, 'tp'), may hold values from -0.125 to 0.125
- norm_gain: float32 [2048], replicated, may hold values from 0.1 to 1.9
- gate_weight: bfloat16 [8, 2048, 4096], P('sp', None, 'tp'), may hold values from -0.5 to 0.5
- up_weight: bfloat16 [8, 2048, 4096], P('sp', None, 'tp'), may hold values from -0.5 to 0.5
- down_weight: bfloat16 [8, 4096, 2048], P('sp', None, 'tp'), may hold values from -0.01171875 to 0.01171875
- expert_ids: int32 [1536, 2], P('sp'), may hold values from 0 to 7, all different within a row; in each aligned block of 192 rows (0 to 191, 192 to 383, ...) at most 96 rows name the same one
- route_logit: float32 [1536, 2], P('sp'), may hold values from -6 to 6
Outputs:
- updated: bfloat16 [1536, 2048], P('sp', 'tp')
Inputs may be any that keep to these rules, and one draw needn't show every extreme that they name: `expert_ids`: A token's 2 experts differ. The 192 tokens of one index of sp name one expert at most 96 times, a bound that some block reaches on some index.
All inputs are finite; a program needn't handle non-finite values.
Results may differ from a plain program's by a relative error of at most 0.014.
Values may be sent and summed in bfloat16 or wider, within the bound.
A program may use at most 64 MiB of HBM per device.

v0:
```python
import functools
import math

import jax
import jax.numpy as jnp
from jax import lax
from jax.experimental import pallas as pl
from jax.experimental.pallas import tpu as pltpu
from jax.sharding import PartitionSpec as P

D = 2048
QK = 64
SPAN = 64


NORM_EPS = 1e-05
CLAMP_LIMIT = 7.0
SWISH_ALPHA = 1.702
HEAD_KEEP = 0.8
NEG_FILL = -1e30


def attend_kernel(
    sp_size,
    queries,
    own_block,
    diff_scale,
    head_gain,
    attended,
    blocks,
    peak,
    total,
    accum,
    local_sem,
    along_send,
    across_send,
    recv,
):
    me = lax.axis_index("sp")
    rank = lax.axis_index("tp")
    pairs = sp_size // 2
    pair = me // 2
    side = lax.rem(me, 2)
    other = me + 1 - 2 * side
    tokens = queries.shape[0]
    width = head_gain.shape[1]
    heads = queries.shape[1] // width

    def place(index):
        return {"sp": index, "tp": rank}

    load = pltpu.make_async_copy(own_block, blocks.at[me], local_sem)
    load.start()
    barrier = pltpu.get_barrier_semaphore()

    def greet(index):
        pl.semaphore_signal(
            barrier, inc=1, device_id=place(index), device_id_type=pl.DeviceIdType.MESH
        )

    greet(other)

    @pl.when(pair > 0)
    def _():
        greet(me - 2)

    @pl.when(pair < pairs - 1)
    def _():
        greet(me + 2)

    pl.semaphore_wait(barrier, 1 + jnp.minimum(pair, 1) + jnp.minimum(pairs - 1 - pair, 1))
    peak[...] = jnp.full(peak.shape, NEG_FILL, jnp.float32)
    total[...] = jnp.zeros(total.shape, jnp.float32)
    accum[...] = jnp.zeros(accum.shape, jnp.float32)
    load.wait()

    def hand_on(block, send, back, target):
        return pltpu.make_async_remote_copy(
            src_ref=blocks.at[block],
            dst_ref=blocks.at[block],
            send_sem=send.at[back],
            recv_sem=recv.at[block],
            device_id=place(target),
            device_id_type=pl.DeviceIdType.MESH,
        )

    def compute(block):
        row = me * tokens + lax.broadcasted_iota(jnp.int32, (tokens, tokens), 0)
        col = block * tokens + lax.broadcasted_iota(jnp.int32, (tokens, tokens), 1)
        visible = col // SPAN <= row // SPAN
        for head in range(heads):
            value = blocks[block, 1, :, head * width : (head + 1) * width]
            for half in range(2):
                start = head * width + half * QK
                scores = lax.dot_general(
                    queries[:, start : start + QK],
                    blocks[block, 0, :, start : start + QK],
                    (((1,), (1,)), ((), ())),
                    preferred_element_type=jnp.float32,
                ) * QK ** (-0.5)
                scores = jnp.where(visible, scores, NEG_FILL)
                index = head * 2 + half
                old = peak[index]
                new = jnp.maximum(old, jnp.max(scores, axis=-1, keepdims=True))
                weights = jnp.where(visible, jnp.exp(scores - new), 0.0)
                rescale = jnp.exp(old - new)
                peak[index] = new
                total[index] = total[index] * rescale + jnp.sum(weights, axis=-1, keepdims=True)
                accum[index] = accum[index] * rescale + jnp.dot(
                    weights.astype(jnp.bfloat16), value, preferred_element_type=jnp.float32
                )

    @pl.loop(0, pair + 2)
    def _(back):
        @pl.when(back <= pair)
        def _():
            block = me - 2 * back

            @pl.when(back > 0)
            def _():
                hand_on(block, across_send, back, other).wait_recv()

            @pl.when(pair < pairs - 1)
            def _():
                hand_on(block, along_send, back, me + 2).start()

            @pl.when((back > 0) | (side == 0))
            def _():
                hand_on(block, across_send, back, other).start()

        second = other - 2 * (back - 1)
        use_second = (back >= 2) | ((back == 1) & (side == 1))

        @pl.loop(0, 2)
        def _(which):
            @pl.when((which == 1) & use_second)
            def _():
                hand_on(second, across_send, 0, other).wait_recv()

            @pl.when(((which == 0) & (back <= pair)) | ((which == 1) & use_second))
            def _():
                compute(jnp.where(which == 0, me - 2 * back, second))

    for head in range(heads):
        first = accum[head * 2] / total[head * 2]
        later = accum[head * 2 + 1] / total[head * 2 + 1]
        mixture = first - diff_scale[head] * later
        scale_back = lax.rsqrt(jnp.mean(mixture * mixture, axis=-1, keepdims=True) + NORM_EPS)
        attended[:, head * width : (head + 1) * width] = (
            mixture * scale_back * head_gain[...] * HEAD_KEEP
        ).astype(jnp.bfloat16)

    @pl.loop(0, pair + 1)
    def _(back):
        block = me - 2 * back

        @pl.when(pair < pairs - 1)
        def _():
            hand_on(block, along_send, back, me + 2).wait_send()

        @pl.when((back > 0) | (side == 0))
        def _():
            hand_on(block, across_send, back, other).wait_send()


def run_attention(queries, key_rows, value_rows, diff_scale, head_gain):
    sp_size = lax.axis_size("sp")
    tokens, heads, width = value_rows.shape
    own_block = jnp.stack(
        [key_rows.reshape(tokens, heads * width), value_rows.reshape(tokens, heads * width)]
    )
    dma = pltpu.SemaphoreType.DMA
    vmem = pl.BlockSpec(memory_space=pltpu.VMEM)
    return pl.pallas_call(
        functools.partial(attend_kernel, sp_size),
        out_shape=jax.ShapeDtypeStruct((tokens, heads * width), jnp.bfloat16),
        in_specs=[
            vmem,
            pl.BlockSpec(memory_space=pl.ANY),
            pl.BlockSpec(memory_space=pltpu.SMEM),
            vmem,
        ],
        out_specs=vmem,
        scratch_shapes=[
            pltpu.VMEM((sp_size,) + own_block.shape, jnp.bfloat16),
            pltpu.VMEM((heads * 2, tokens, 1), jnp.float32),
            pltpu.VMEM((heads * 2, tokens, 1), jnp.float32),
            pltpu.VMEM((heads * 2, tokens, width), jnp.float32),
            dma(()),
            dma((sp_size,)),
            dma((sp_size,)),
            dma((sp_size,)),
        ],
        compiler_params=pltpu.CompilerParams(
            collective_id=1, has_side_effects=True, vmem_limit_bytes=32 * 1024 * 1024
        ),
    )(queries.reshape(tokens, heads * width), own_block, diff_scale, head_gain[None])


def expert_kernel(
    sp_size,
    tp_size,
    groups,
    outgoing,
    gate_hbm,
    up_hbm,
    down_hbm,
    returned,
    rows_in,
    hidden,
    result,
    gate,
    up,
    down,
    weight_sem,
    local_sem,
    disp_send,
    disp_recv,
    ret_send,
    ret_recv,
    row_send,
    row_recv,
    hid_send,
    hid_recv,
):
    me = lax.axis_index("sp")
    rank = lax.axis_index("tp")
    parity = lax.rem(rank, 2)
    sibling = rank + 1 - 2 * parity
    chips = tp_size // 2
    chip = rank // 2
    span = sp_size // groups
    cap = outgoing.shape[1]
    feats = outgoing.shape[2]
    units = gate.shape[1]
    columns = down.shape[1]

    weights = [
        pltpu.make_async_copy(src, dst, weight_sem.at[i])
        for i, (src, dst) in enumerate(((gate_hbm, gate), (up_hbm, up), (down_hbm, down)))
    ]
    for copy in weights:
        copy.start()

    def peer_rank(step):
        return lax.rem(chip + step, chips) * 2 + parity

    barrier = pltpu.get_barrier_semaphore()
    for step in range(1, sp_size):
        pl.semaphore_signal(
            barrier,
            inc=1,
            device_id={"sp": lax.rem(me + step, sp_size), "tp": rank},
            device_id_type=pl.DeviceIdType.MESH,
        )
    for step in range(1, chips):
        pl.semaphore_signal(
            barrier,
            inc=1,
            device_id={"sp": me, "tp": peer_rank(step)},
            device_id_type=pl.DeviceIdType.MESH,
        )
    pl.semaphore_signal(
        barrier,
        inc=1,
        device_id={"sp": me, "tp": sibling},
        device_id_type=pl.DeviceIdType.MESH,
    )
    pl.semaphore_wait(barrier, sp_size - 1 + chips)

    def slot(step):
        return rows_in.at[step // span, rank, pl.ds((step % span) * cap, cap)]

    def dispatch(step):
        expert = lax.rem(me + sp_size - step, sp_size)
        return pltpu.make_async_remote_copy(
            src_ref=outgoing.at[expert],
            dst_ref=slot(step),
            send_sem=disp_send.at[step],
            recv_sem=disp_recv.at[step],
            device_id={"sp": expert, "tp": rank},
            device_id_type=pl.DeviceIdType.MESH,
        )

    own_in = pltpu.make_async_copy(outgoing.at[me], slot(0), local_sem.at[0])
    own_in.start()
    for step in range(1, sp_size):
        dispatch(step).start()

    def piece(buffer, send, recv, group, owner, target, send_slot):
        return pltpu.make_async_remote_copy(
            src_ref=buffer.at[group, owner],
            dst_ref=buffer.at[group, owner],
            send_sem=send.at[group, send_slot],
            recv_sem=recv.at[group, owner],
            device_id={"sp": me, "tp": target},
            device_id_type=pl.DeviceIdType.MESH,
        )

    def spread(buffer, send, recv, group):
        for step in range(1, chips):
            target = peer_rank(step)
            piece(buffer, send, recv, group, rank, target, target).start()
        piece(buffer, send, recv, group, rank, sibling, sibling).start()

    def collect(buffer, send, recv, group):
        for step in range(1, chips):
            owner = peer_rank(step)
            forward = piece(buffer, send, recv, group, owner, sibling, owner + 1 - 2 * parity)
            forward.wait_recv()
            forward.start()
        for step in range(chips):
            owner = peer_rank(step) + 1 - 2 * parity
            piece(buffer, send, recv, group, owner, sibling, sibling).wait_recv()

    unit_tile = math.gcd(units, 256)
    column_tile = math.gcd(columns, 256)

    def spread_rows(group):
        for place in range(span):
            def arrived(place=place):
                step = group * span + place
                pltpu.make_async_remote_copy(
                    src_ref=outgoing.at[0],
                    dst_ref=rows_in.at[group, rank, pl.ds(place * cap, cap)],
                    send_sem=disp_send.at[step],
                    recv_sem=disp_recv.at[step],
                    device_id={"sp": me, "tp": sibling},
                    device_id_type=pl.DeviceIdType.MESH,
                ).wait_recv()

            if place == 0:
                @pl.when(group == 0)
                def _():
                    own_in.wait()

                pl.when(group > 0)(arrived)
            else:
                arrived()
        spread(rows_in, row_send, row_recv, group)

    def run_up(group):
        collect(rows_in, row_send, row_recv, group)

        @pl.when(group == 0)
        def _():
            weights[0].wait()
            weights[1].wait()

        @pl.loop(0, units // unit_tile)
        def _(tile):
            cols = pl.ds(pl.multiple_of(tile * unit_tile, unit_tile), unit_tile)
            pre_gate = 0.0
            pre_up = 0.0
            for part in range(tp_size):
                block = rows_in[group, part]
                depth = pl.ds(part * feats, feats)
                pre_gate += jnp.dot(block, gate[depth, cols], preferred_element_type=jnp.float32)
                pre_up += jnp.dot(block, up[depth, cols], preferred_element_type=jnp.float32)
            capped = jnp.minimum(pre_gate, CLAMP_LIMIT)
            linear = jnp.clip(pre_up, -CLAMP_LIMIT, CLAMP_LIMIT)
            value = capped * jax.nn.sigmoid(SWISH_ALPHA * capped) * (linear + 1.0)
            hidden[group, rank, :, cols] = value.astype(jnp.bfloat16)

        spread(hidden, hid_send, hid_recv, group)

    def give_back(step):
        source = lax.rem(me + step, sp_size)
        return pltpu.make_async_remote_copy(
            src_ref=result.at[step // span, pl.ds((step % span) * cap, cap)],
            dst_ref=returned.at[me],
            send_sem=ret_send.at[step],
            recv_sem=ret_recv.at[step],
            device_id={"sp": source, "tp": rank},
            device_id_type=pl.DeviceIdType.MESH,
        )

    own_out = pltpu.make_async_copy(result.at[0, pl.ds(0, cap)], returned.at[me], local_sem.at[1])

    def run_down(group):
        collect(hidden, hid_send, hid_recv, group)

        @pl.when(group == 0)
        def _():
            weights[2].wait()

        @pl.loop(0, columns // column_tile)
        def _(tile):
            cols = pl.ds(pl.multiple_of(tile * column_tile, column_tile), column_tile)
            total = 0.0
            for part in range(tp_size):
                total += jnp.dot(
                    hidden[group, part],
                    down[pl.ds(part * units, units), cols],
                    preferred_element_type=jnp.float32,
                )
            result[group, :, cols] = total.astype(jnp.bfloat16)

        for place in range(span):
            if place == 0:
                @pl.when(group == 0)
                def _():
                    own_out.start()

                @pl.when(group > 0)
                def _():
                    give_back(group * span).start()
            else:
                give_back(group * span + place).start()

    @pl.loop(0, groups + 2)
    def _(turn):
        @pl.when(turn < groups)
        def _():
            spread_rows(turn)

        @pl.when((turn >= 1) & (turn < groups + 1))
        def _():
            run_up(turn - 1)

        @pl.when(turn >= 2)
        def _():
            run_down(turn - 2)

    own_out.wait()
    for step in range(1, sp_size):
        dispatch(step).wait_send()
    for step in range(1, sp_size):
        back = give_back(step)
        back.wait_send()
        pltpu.make_async_remote_copy(
            src_ref=result.at[0, pl.ds(0, cap)],
            dst_ref=returned.at[lax.rem(me + sp_size - step, sp_size)],
            send_sem=ret_send.at[step],
            recv_sem=ret_recv.at[step],
            device_id={"sp": lax.rem(me + step, sp_size), "tp": rank},
            device_id_type=pl.DeviceIdType.MESH,
        ).wait_recv()

    @pl.loop(0, groups)
    def _(group):
        for buffer, send, recv in ((rows_in, row_send, row_recv), (hidden, hid_send, hid_recv)):
            for step in range(1, chips):
                target = peer_rank(step)
                piece(buffer, send, recv, group, rank, target, target).wait_send()
                other = target + 1 - 2 * parity
                piece(buffer, send, recv, group, target, sibling, other).wait_send()
            piece(buffer, send, recv, group, rank, sibling, sibling).wait_send()


def run_experts(outgoing, gate_weight, up_weight, down_weight):
    sp_size, cap, feats = outgoing.shape
    tp_size = lax.axis_size("tp")
    groups = math.gcd(sp_size, 4)
    rows = sp_size // groups * cap
    units = gate_weight.shape[1]
    columns = down_weight.shape[1]
    dma = pltpu.SemaphoreType.DMA
    return pl.pallas_call(
        functools.partial(expert_kernel, sp_size, tp_size, groups),
        out_shape=jax.ShapeDtypeStruct((sp_size, cap, columns), jnp.bfloat16),
        in_specs=[pl.BlockSpec(memory_space=pltpu.VMEM)]
        + [pl.BlockSpec(memory_space=pl.ANY)] * 3,
        out_specs=pl.BlockSpec(memory_space=pl.ANY),
        scratch_shapes=[
            pltpu.VMEM((groups, tp_size, rows, feats), jnp.bfloat16),
            pltpu.VMEM((groups, tp_size, rows, units), jnp.bfloat16),
            pltpu.VMEM((groups, rows, columns), jnp.bfloat16),
            pltpu.VMEM(gate_weight.shape, jnp.bfloat16),
            pltpu.VMEM(up_weight.shape, jnp.bfloat16),
            pltpu.VMEM(down_weight.shape, jnp.bfloat16),
            dma((3,)),
            dma((2,)),
            dma((sp_size,)),
            dma((sp_size,)),
            dma((sp_size,)),
            dma((sp_size,)),
            dma((groups, tp_size)),
            dma((groups, tp_size)),
            dma((groups, tp_size)),
            dma((groups, tp_size)),
        ],
        compiler_params=pltpu.CompilerParams(
            collective_id=0, has_side_effects=True, vmem_limit_bytes=48 * 1024 * 1024
        ),
    )(outgoing, gate_weight, up_weight, down_weight)


def local(
    residual,
    queries,
    key_rows,
    value_rows,
    diff_scale,
    head_gain,
    out_weight,
    norm_gain,
    gate_weight,
    up_weight,
    down_weight,
    expert_ids,
    route_logit,
):
    tokens_here = queries.shape[0]
    attended = run_attention(queries, key_rows, value_rows, diff_scale, head_gain)
    column_width = out_weight.shape[1]
    gathered = lax.all_gather(attended, "tp", axis=0)
    projected = jnp.einsum(
        "rtv,rvd->td",
        gathered,
        out_weight.reshape(gathered.shape[0], -1, column_width),
        preferred_element_type=jnp.float32,
    )
    after_mixer = (residual.astype(jnp.float32) + projected).astype(jnp.bfloat16)
    mixer_float = after_mixer.astype(jnp.float32)
    partial_value = jnp.sum(mixer_float * mixer_float, axis=-1)
    square_total = lax.psum(partial_value, "tp")
    gain_slice = lax.dynamic_slice_in_dim(
        norm_gain, lax.axis_index("tp") * column_width, column_width, 0
    )
    normed = (mixer_float * lax.rsqrt(square_total / D + NORM_EPS)[:, None] * gain_slice).astype(
        jnp.bfloat16
    )
    experts = lax.axis_size("sp")
    top_count = expert_ids.shape[1]
    capacity = -(-(2 * tokens_here * top_count // experts) // 16) * 16
    chosen = expert_ids.reshape(-1)
    order = jnp.arange(chosen.shape[0], dtype=jnp.int32)
    earlier = (chosen[:, None] == chosen[None, :]) & (order[None, :] < order[:, None])
    rank_in = jnp.sum(earlier.astype(jnp.int32), axis=1)
    slot_index = (chosen * capacity + rank_in).reshape(tokens_here, top_count)
    slots = jnp.arange(experts * capacity, dtype=jnp.int32)
    holds = [slot_index[:, k][:, None] == slots[None, :] for k in range(top_count)]
    holds_any = functools.reduce(jnp.logical_or, holds)
    outgoing = (
        jnp.einsum(
            "ts,td->sd",
            holds_any.astype(jnp.bfloat16),
            normed,
            preferred_element_type=jnp.float32,
        )
        .astype(jnp.bfloat16)
        .reshape(experts, capacity, normed.shape[1])
    )
    returned_rows = run_experts(outgoing, gate_weight[0], up_weight[0], down_weight[0])
    flat_rows = returned_rows.reshape(experts * capacity, -1)
    weights = jax.nn.softmax(route_logit, axis=-1)
    routed = 0.0
    for k in range(top_count):
        picked = jnp.dot(
            holds[k].astype(jnp.bfloat16), flat_rows, preferred_element_type=jnp.float32
        )
        routed = routed + picked * weights[:, k : k + 1]
    return (mixer_float + routed).astype(jnp.bfloat16)


def solution(mesh):
    return jax.shard_map(
        local,
        mesh=mesh,
        in_specs=(
            P("sp", "tp"),
            P("sp", "tp", None),
            P("sp", "tp", None),
            P("sp", "tp", None),
            P("tp"),
            P(),
            P(None, "tp"),
            P(),
            P("sp", None, "tp"),
            P("sp", None, "tp"),
            P("sp", None, "tp"),
            P("sp", None),
            P("sp", None),
        ),
        out_specs=P("sp", "tp"),
        check_vma=False,
    )
```

profile of v0, /device:TPU:0, one launch (start us, length us, event | category | flops | bytes accessed | tf_op | source)
XLA Modules:
  0.0 144.3 jit_solution(14924185588422604546)
XLA Ops:
  0.0 0.0 copy-start
  0.0 0.0 copy-start.4
  0.0 0.9 dynamic_slice.3
  0.9 1.0 stack_reshape.6
  1.9 1.0 stack_reshape.7
  3.0 1.0 copy.27
  3.9 0.0 copy-start.2
  4.0 0.6 copy-done.2
  4.6 0.0 copy-start.3
  4.6 0.7 copy-done.3
  5.3 12.6 %shard_map.127 = bf16[192,512]{1,0:T(8,128)(2,1)S(1)} custom-call(bf16[192,512]{1,0:T(8,128)(2,1)S(1)} %bitcast.33, bf16[2,192,512]{2,1,0:T(8,128)(2,1)S(1)} %pad_maximum_fusion.own_block, f32[4]{0:T(128)S(1)} %copy-done.2, f32[1,128]{1,0:T(1,128)S(1)} %bitcast.34), custom_call_target="tpu_custom_call" | custom-call | tf_op jit(solution)/shard_map/pallas_call | solution.py:174
  17.8 0.0 copy-start.6
  17.9 8.6 %all-gather = bf16[768,512]{1,0:T(8,128)(2,1)S(1)} all-gather(bf16[192,512]{1,0:T(8,128)(2,1)S(1)} %shard_map.127), channel_id=2, replica_groups=mesh['sp'=8,'tp'=4] {'tp'}, dimensions={0}, use_global_device_ids=true | all-gather | bytes 983040 | tf_op jit(solution)/shard_map/all_gather | solution.py:507
  26.5 0.0 copy-done
  26.5 0.0 copy-done.4
  26.5 0.7 multiply_reduce_fusion
  27.2 0.0 copy-done.6
  27.2 0.1 copy.23
  27.3 0.1 eq.45
  27.4 0.2 convert_reduce_fusion
  27.7 0.1 reduce_sum.30
  27.8 0.1 copy.24
  27.9 6.1 %psum.7 = f32[192]{0:T(256)S(1)} all-reduce(f32[192]{0:T(256)S(1)} %get-tuple-element.9), channel_id=1, replica_groups=mesh['sp'=8,'tp'=4] {'tp'}, use_global_device_ids=true, to_apply=%region_2.0 | all-reduce | flops 192 | bytes 1536 | tf_op jit(solution)/shard_map/psum | solution.py:517
  34.1 0.5 convolution_convert_fusion
  34.6 0.0 copy-start.1
  34.6 2.2 %copy-done.1 = bf16[1,2048,1024]{2,1,0:T(8,128)(2,1)S(1)} copy-done((bf16[1,2048,1024]{2,1,0:T(8,128)(2,1)S(1)}, bf16[1,2048,1024]{2,1,0:T(8,128)(2,1)}, u32[]{:S(2)}) %copy-start.1) | copy-done | bytes 4194328
  36.8 0.0 copy-start.5
  36.8 106.0 %shard_map.128 = bf16[8,96,512]{2,1,0:T(8,128)(2,1)S(1)} custom-call(bf16[8,96,512]{2,1,0:T(8,128)(2,1)S(1)} %bitcast.32, bf16[2048,1024]{1,0:T(8,128)(2,1)S(1)} %bitcast.31, bf16[2048,1024]{1,0:T(8,128)(2,1)} %bitcast.35, bf16[4096,512]{1,0:T(8,128)(2,1)} %bitcast.36), custom_call_target="tpu_custom_call" | custom-call | tf_op jit(solution)/shard_map/pallas_call | solution.py:459
  142.8 0.0 copy-done.5
  142.9 0.4 convolution_multiply_fusion.1
  143.3 1.1 fusion.3
  (8 shorter events, 0.1 us)
Async XLA Ops:
  0.0 26.5 %copy-start = (bf16[2048,512]{1,0:T(8,128)(2,1)S(1)}, bf16[2048,512]{1,0:T(8,128)(2,1)}, u32[]{:S(2)}) copy-start(bf16[2048,512]{1,0:T(8,128)(2,1)} %param.19) | copy-start | bytes 6291460
  0.0 26.5 %copy-start.4 = (bf16[192,512]{1,0:T(8,128)(2,1)S(1)}, bf16[192,512]{1,0:T(8,128)(2,1)}, u32[]{:S(2)}) copy-start(bf16[192,512]{1,0:T(8,128)(2,1)} %param.13) | copy-start | bytes 589828
  3.9 0.7 copy-start.2
  4.6 0.7 copy-start.3
  17.8 9.3 %copy-start.6 = (s32[192,2]{0,1:T(2,128)S(1)}, s32[192,2]{0,1:T(2,128)}, u32[]{:S(2)}) copy-start(s32[192,2]{0,1:T(2,128)} %param.24) | copy-start | bytes 4612
  34.6 2.2 %copy-start.1 = (bf16[1,2048,1024]{2,1,0:T(8,128)(2,1)S(1)}, bf16[1,2048,1024]{2,1,0:T(8,128)(2,1)}, u32[]{:S(2)}) copy-start(bf16[1,2048,1024]{2,1,0:T(8,128)(2,1)} %param.21) | copy-start | bytes 12582916
  36.8 106.0 %copy-start.5 = (f32[192,2]{0,1:T(2,128)S(1)}, f32[192,2]{0,1:T(2,128)}, u32[]{:S(2)}) copy-start(f32[192,2]{0,1:T(2,128)} %param.25) | copy-start | bytes 4612
where the time goes:
time: 145 us; the launch traced here: 144 us
  Pallas kernels  119 us (82%)
  blocking collectives  14.7 us (10%)
  local copies, waits for them, and re-layouts  7.88 us (5%)
  matrix products  2.65 us (2%)
    pallas_call x1, Pallas kernels, run_experts(): pl.pallas_call(functools.partial(expert_kernel, sp_size, tp_size, groups)...  106 us
    pallas_call x1, Pallas kernels, run_attention(): pl.pallas_call(functools.partial(attend_kernel, sp_size), out_shape=jax.S...  12.6 us
    all_gather x1, blocking collectives, local(): gathered = lax.all_gather(attended, 'tp', axis=0)  8.63 us
    psum x1, blocking collectives, local(): square_total = lax.psum(partial_value, 'tp')  6.12 us
    unnamed x16, local copies, waits for them, and re-layouts  4.58 us

commit v1 on v0

v1 whole, which is shorter than its diff:
```python
import functools
import math

import jax
import jax.numpy as jnp
from jax import lax
from jax.experimental import pallas as pl
from jax.experimental.pallas import tpu as pltpu
from jax.sharding import PartitionSpec as P

D = 2048
QK = 64
SPAN = 64


NORM_EPS = 1e-05
CLAMP_LIMIT = 7.0
SWISH_ALPHA = 1.702
HEAD_KEEP = 0.8
NEG_FILL = -1e30
MESH = pl.DeviceIdType.MESH
F32 = jnp.float32
BF16 = jnp.bfloat16


def layer_kernel(
    sp_size,
    tp_size,
    groups,
    cap,
    early,
    residual,
    queries,
    own_block,
    diff_scale,
    head_gain,
    out_hbm,
    norm_gain,
    gate_hbm,
    up_hbm,
    down_hbm,
    expert_ids,
    route_logit,
    updated,
    scaled,
    blocks,
    peak,
    total,
    accum,
    heads_all,
    out_w,
    mixer,
    places,
    outgoing,
    rows_in,
    normed,
    hidden,
    down_part,
    own_sum,
    part_send,
    part_recv,
    result,
    returned,
    gate,
    up,
    weight_sem,
    block_sem,
    along_send,
    across_send,
    kv_recv,
    down_send,
    down_recv,
    att_send,
    att_recv,
    disp_send,
    disp_recv,
    row_send,
    row_recv,
    hid_send,
    hid_recv,
    sum_send,
    sum_recv,
    ret_send,
    ret_recv,
):
    me = lax.axis_index("sp")
    rank = lax.axis_index("tp")
    parity = lax.rem(rank, 2)
    sibling = rank + 1 - 2 * parity
    chips = tp_size // 2
    chip = rank // 2
    span = sp_size // groups
    rows = span * cap
    tokens = queries.shape[0]
    width = head_gain.shape[1]
    heads = queries.shape[1] // width
    feats = residual.shape[1]
    units = gate.shape[1]
    columns = feats
    tops = expert_ids.shape[1]

    def at(index):
        return {"sp": index, "tp": rank}

    def beside(target):
        return {"sp": me, "tp": target}

    def peer_rank(step):
        return lax.rem(chip + step, chips) * 2 + parity

    def remote(src, dst, send, recv, device):
        return pltpu.make_async_remote_copy(
            src_ref=src,
            dst_ref=dst,
            send_sem=send,
            recv_sem=recv,
            device_id=device,
            device_id_type=MESH,
        )

    load = pltpu.make_async_copy(own_block, blocks.at[me], block_sem)
    load.start()
    pieces = down_send.shape[1]
    chunk = 2 * units // pieces
    weights = [
        pltpu.make_async_copy(out_hbm, out_w, weight_sem.at[0]),
        pltpu.make_async_copy(gate_hbm, gate, weight_sem.at[1]),
        pltpu.make_async_copy(up_hbm, up, weight_sem.at[2]),
        pltpu.make_async_copy(
            down_hbm.at[pl.ds(chip * 2 * units, 2 * units)], down_part.at[chip], weight_sem.at[3]
        ),
    ]
    for copy in weights:
        copy.start()

    barrier = pltpu.get_barrier_semaphore()
    for step in range(1, sp_size):
        pl.semaphore_signal(
            barrier, inc=1, device_id=at(lax.rem(me + step, sp_size)), device_id_type=MESH
        )
    for step in range(1, chips):
        pl.semaphore_signal(barrier, inc=1, device_id=beside(peer_rank(step)), device_id_type=MESH)
    pl.semaphore_signal(barrier, inc=1, device_id=beside(sibling), device_id_type=MESH)

    scaled[...] = (queries[...].astype(F32) * QK ** (-0.5)).astype(BF16)
    total[...] = jnp.zeros(total.shape, F32)
    accum[...] = jnp.zeros(accum.shape, F32)
    peak[...] = jnp.full(peak.shape, NEG_FILL, F32)

    lane = lax.broadcasted_iota(jnp.int32, (tokens, 128), 1)
    named = [lane == expert_ids[:, k : k + 1] for k in range(tops)]
    both = functools.reduce(jnp.logical_or, named).astype(F32).astype(BF16)
    before = (
        lax.broadcasted_iota(jnp.int32, (tokens, tokens), 1)
        < lax.broadcasted_iota(jnp.int32, (tokens, tokens), 0)
    ).astype(F32).astype(BF16)
    earlier = jnp.dot(before, both, preferred_element_type=F32)
    for k in range(tops):
        order = jnp.sum(jnp.where(named[k], earlier, 0.0), axis=1, keepdims=True)
        step_of = lax.rem(me + sp_size - expert_ids[:, k : k + 1], sp_size)
        places[:, k : k + 1] = step_of * cap + order.astype(jnp.int32)

    pl.semaphore_wait(barrier, sp_size - 1 + chips)

    def down_piece(step, piece):
        target = lax.rem(chip + step, chips)
        return remote(
            down_hbm.at[pl.ds(target * 2 * units + piece * chunk, chunk)],
            down_part.at[chip, pl.ds(piece * chunk, chunk)],
            down_send.at[step - 1, piece],
            down_recv.at[chip, piece],
            beside(target * 2 + parity),
        )

    def send_down(first, last):
        for step in range(1, chips):
            @pl.loop(first, last)
            def _(piece):
                down_piece(step, piece).start()

    load.wait()

    pairs = sp_size // 2
    pair = me // 2
    side = lax.rem(me, 2)
    other = me + 1 - 2 * side

    def hand_on(block, send, back, target):
        return remote(
            blocks.at[block], blocks.at[block], send.at[back], kv_recv.at[block], at(target)
        )

    def attend(block, masked):
        if masked:
            row = me * tokens + lax.broadcasted_iota(jnp.int32, (tokens, tokens), 0)
            col = block * tokens + lax.broadcasted_iota(jnp.int32, (tokens, tokens), 1)
            visible = col // SPAN <= row // SPAN
        for head in range(heads):
            value = blocks[block, 1, :, head * width : (head + 1) * width]
            for half in range(2):
                start = head * width + half * QK
                scores = lax.dot_general(
                    scaled[:, start : start + QK],
                    blocks[block, 0, :, start : start + QK],
                    (((1,), (1,)), ((), ())),
                    preferred_element_type=F32,
                )
                if masked:
                    scores = jnp.where(visible, scores, NEG_FILL)
                index = head * 2 + half
                old = peak[index]
                new = jnp.maximum(old, jnp.max(scores, axis=-1, keepdims=True))
                exps = jnp.exp(scores - new)
                if masked:
                    exps = jnp.where(visible, exps, 0.0)
                rescale = jnp.exp(old - new)
                peak[index] = new
                total[index] = total[index] * rescale + jnp.sum(exps, axis=-1, keepdims=True)
                accum[index] = accum[index] * rescale + jnp.dot(
                    exps.astype(BF16), value, preferred_element_type=F32
                )

    plain_blocks = tokens % SPAN == 0

    @pl.loop(0, pair + 2)
    def _(back):
        @pl.when(back <= pair)
        def _():
            block = me - 2 * back

            @pl.when(back > 0)
            def _():
                hand_on(block, across_send, back, other).wait_recv()

            @pl.when(pair < pairs - 1)
            def _():
                hand_on(block, along_send, back, me + 2).start()

            @pl.when((back > 0) | (side == 0))
            def _():
                hand_on(block, across_send, back, other).start()

        @pl.when(back == 0)
        def _():
            send_down(0, early)
            attend(me, True)

        second = other - 2 * (back - 1)
        use_second = (back >= 2) | ((back == 1) & (side == 1))

        @pl.loop(0, 2)
        def _(which):
            @pl.when((which == 1) & use_second)
            def _():
                hand_on(second, across_send, 0, other).wait_recv()

            @pl.when(((which == 0) & (back > 0) & (back <= pair)) | ((which == 1) & use_second))
            def _():
                attend(jnp.where(which == 0, me - 2 * back, second), not plain_blocks)

    def piece(buffer, send, recv, owner, target, send_slot):
        return remote(
            buffer.at[owner],
            buffer.at[owner],
            send.at[send_slot],
            recv.at[owner],
            beside(target),
        )

    def spread(buffer, send, recv):
        for step in range(1, chips):
            target = peer_rank(step)
            piece(buffer, send, recv, rank, target, target).start()
        piece(buffer, send, recv, rank, sibling, sibling).start()

    def forward(buffer, send, recv, step):
        owner = peer_rank(step)
        onward = piece(buffer, send, recv, owner, sibling, owner + 1 - 2 * parity)
        onward.wait_recv()
        onward.start()

    def collect(buffer, send, recv):
        for step in range(1, chips):
            forward(buffer, send, recv, step)
        for step in range(chips):
            owner = peer_rank(step) + 1 - 2 * parity
            piece(buffer, send, recv, owner, sibling, sibling).wait_recv()

    def settle(buffer, send, recv):
        for step in range(1, chips):
            target = peer_rank(step)
            piece(buffer, send, recv, rank, target, target).wait_send()
            piece(buffer, send, recv, target, sibling, target + 1 - 2 * parity).wait_send()
        piece(buffer, send, recv, rank, sibling, sibling).wait_send()

    for head in range(heads):
        first = accum[head * 2] / total[head * 2]
        later = accum[head * 2 + 1] / total[head * 2 + 1]
        mixture = first - diff_scale[head] * later
        scale_back = lax.rsqrt(jnp.mean(mixture * mixture, axis=-1, keepdims=True) + NORM_EPS)
        heads_all[rank, :, head * width : (head + 1) * width] = (
            mixture * scale_back * head_gain[...] * HEAD_KEEP
        ).astype(BF16)
    spread(heads_all, att_send, att_recv)
    send_down(early, pieces)
    weights[0].wait()

    def project(owner):
        return jnp.dot(
            heads_all[owner],
            out_w[pl.ds(pl.multiple_of(owner * heads * width, heads * width), heads * width)],
            preferred_element_type=F32,
        )

    sums = own_sum.at[0, pl.ds(0, tokens)]
    sums[...] = residual[...].astype(F32) + project(rank)
    collect(heads_all, att_send, att_recv)
    for step in range(chips):
        owner = peer_rank(step) + 1 - 2 * parity
        sums[...] += project(owner)
        if step > 0:
            sums[...] += project(peer_rank(step))
    mixer[...] = sums[...].astype(BF16)

    def slots_of(first, count):
        slot = first + lax.broadcasted_iota(jnp.int32, (tokens, count), 1)
        return [
            (slot == places[:, k : k + 1]).astype(F32).astype(BF16) for k in range(tops)
        ]

    def chosen_rows(step):
        held = functools.reduce(jnp.add, slots_of(step * cap, cap))
        return lax.dot_general(
            held, mixer[...], (((0,), (0,)), ((), ())), preferred_element_type=F32
        ).astype(BF16)

    def dispatch(step):
        expert = lax.rem(me + sp_size - step, sp_size)
        return remote(
            outgoing.at[step],
            rows_in.at[step // span, rank, pl.ds(lax.rem(step, span) * cap, cap)],
            disp_send.at[step],
            disp_recv.at[step],
            at(expert),
        )

    rows_in[0, rank, pl.ds(0, cap), :] = chosen_rows(0)

    @pl.loop(1, sp_size)
    def _(step):
        outgoing[step] = chosen_rows(step)
        dispatch(step).start()

    unit_tile = math.gcd(units, 256)
    column_tile = math.gcd(columns, 256)

    def spread_rows(group):
        for place in range(span):
            step = group * span + place
            arrived = remote(
                outgoing.at[0],
                rows_in.at[group, rank, pl.ds(place * cap, cap)],
                disp_send.at[step],
                disp_recv.at[step],
                beside(sibling),
            )
            if place == 0:
                @pl.when(group > 0)
                def _():
                    arrived.wait_recv()
            else:
                arrived.wait_recv()
        spread(rows_in.at[group], row_send.at[group], row_recv.at[group])

    def hidden_copy(group):
        return remote(
            hidden.at[group, parity],
            hidden.at[group, parity],
            hid_send.at[group],
            hid_recv.at[group],
            beside(sibling),
        )

    def run_up(group):
        collect(rows_in.at[group], row_send.at[group], row_recv.at[group])

        @pl.when(group == 0)
        def _():
            weights[1].wait()
            weights[2].wait()

        square = 0.0
        for part in range(tp_size):
            value = rows_in[group, part].astype(F32)
            square += jnp.sum(value * value, axis=-1, keepdims=True)
        scale_back = lax.rsqrt(square / (tp_size * feats) + NORM_EPS)
        for part in range(tp_size):
            depth = slice(part * feats, (part + 1) * feats)
            normed[:, depth] = (
                rows_in[group, part].astype(F32) * scale_back * norm_gain[:, depth]
            ).astype(BF16)

        @pl.loop(0, units // unit_tile)
        def _(tile):
            cols = pl.ds(pl.multiple_of(tile * unit_tile, unit_tile), unit_tile)
            pre_gate = jnp.dot(normed[...], gate[:, cols], preferred_element_type=F32)
            pre_up = jnp.dot(normed[...], up[:, cols], preferred_element_type=F32)
            capped = jnp.minimum(pre_gate, CLAMP_LIMIT)
            linear = jnp.clip(pre_up, -CLAMP_LIMIT, CLAMP_LIMIT)
            value = capped * jax.nn.sigmoid(SWISH_ALPHA * capped) * (linear + 1.0)
            hidden[group, parity, :, cols] = value.astype(BF16)

        hidden_copy(group).start()

    def sum_copy(group, step):
        target = lax.rem(chip + step, chips)
        return remote(
            part_send.at[group, step - 1],
            part_recv.at[group, step - 1],
            sum_send.at[group, step - 1],
            sum_recv.at[group, step - 1],
            beside(target * 2 + parity),
        )

    def part_sum(group, block, cols):
        value = 0.0
        for core in range(2):
            value += jnp.dot(
                hidden[group, core],
                down_part[block, core * units : (core + 1) * units, cols],
                preferred_element_type=F32,
            )
        return value

    def run_down(group):
        remote(
            hidden.at[group, 1 - parity],
            hidden.at[group, 1 - parity],
            hid_send.at[group],
            hid_recv.at[group],
            beside(sibling),
        ).wait_recv()

        @pl.when(group == 0)
        def _():
            weights[3].wait()
            for step in range(1, chips):
                source = lax.rem(chip + step, chips)

                @pl.loop(0, pieces)
                def _(index):
                    remote(
                        down_part.at[source, pl.ds(index * chunk, chunk)],
                        down_part.at[source, pl.ds(index * chunk, chunk)],
                        down_send.at[step - 1, index],
                        down_recv.at[source, index],
                        beside(sibling),
                    ).wait_recv()

        for step in range(1, chips):
            @pl.loop(0, columns // column_tile)
            def _(tile):
                cols = pl.ds(pl.multiple_of(tile * column_tile, column_tile), column_tile)
                part_send[group, step - 1, :, cols] = part_sum(
                    group, lax.rem(chip + step, chips), cols
                ).astype(BF16)

            sum_copy(group, step).start()

        @pl.loop(0, columns // column_tile)
        def _(tile):
            cols = pl.ds(pl.multiple_of(tile * column_tile, column_tile), column_tile)
            own_sum[lax.rem(group, 2), pl.ds(0, rows), cols] = part_sum(group, chip, cols)

    def give_back(group, place):
        step = group * span + place
        return remote(
            result.at[group, pl.ds(place * cap, cap)],
            returned.at[group, pl.ds(place * cap, cap)],
            ret_send.at[step],
            ret_recv.at[step],
            at(lax.rem(me + step, sp_size)),
        )

    def finish(group):
        value = own_sum[lax.rem(group, 2), pl.ds(0, rows), :]
        for step in range(1, chips):
            sum_copy(group, step).wait_recv()
            value += part_recv[group, step - 1].astype(F32)
        result[group] = value.astype(BF16)
        for place in range(span):
            if place == 0:
                @pl.when(group == 0)
                def _():
                    returned[0, pl.ds(0, cap), :] = result[0, pl.ds(0, cap), :]

                @pl.when(group > 0)
                def _():
                    give_back(group, 0).start()
            else:
                give_back(group, place).start()

    @pl.loop(0, groups + 3)
    def _(turn):
        @pl.when(turn < groups)
        def _():
            spread_rows(turn)

        @pl.when((turn >= 1) & (turn < groups + 1))
        def _():
            run_up(turn - 1)

        @pl.when((turn >= 3))
        def _():
            finish(turn - 3)

        @pl.when((turn >= 2) & (turn < groups + 2))
        def _():
            run_down(turn - 2)

    peak_logit = jnp.max(route_logit[...], axis=-1, keepdims=True)
    shares = jnp.exp(route_logit[...] - peak_logit)
    shares = shares / jnp.sum(shares, axis=-1, keepdims=True)
    back_sum = own_sum.at[0, pl.ds(0, tokens)]
    back_sum[...] = mixer[...].astype(F32)

    @pl.loop(0, groups)
    def _(group):
        for place in range(span):
            if place == 0:
                @pl.when(group > 0)
                def _():
                    give_back(group, 0).wait_recv()
            else:
                give_back(group, place).wait_recv()
        routed = 0.0
        for k, held in enumerate(slots_of(group * rows, rows)):
            picked = jnp.dot(held, returned[group], preferred_element_type=F32)
            routed += picked * shares[:, k : k + 1]
        back_sum[...] += routed

    updated[...] = back_sum[...].astype(BF16)

    @pl.loop(0, pair + 1)
    def _(back):
        block = me - 2 * back

        @pl.when(pair < pairs - 1)
        def _():
            hand_on(block, along_send, back, me + 2).wait_send()

        @pl.when((back > 0) | (side == 0))
        def _():
            hand_on(block, across_send, back, other).wait_send()

    for step in range(1, chips):
        @pl.loop(0, pieces)
        def _(index):
            down_piece(step, index).wait_send()

    settle(heads_all, att_send, att_recv)

    @pl.loop(1, sp_size)
    def _(step):
        dispatch(step).wait_send()

    @pl.loop(0, groups)
    def _(group):
        settle(rows_in.at[group], row_send.at[group], row_recv.at[group])
        hidden_copy(group).wait_send()
        for step in range(1, chips):
            sum_copy(group, step).wait_send()
        for place in range(span):
            if place == 0:
                @pl.when(group > 0)
                def _():
                    give_back(group, 0).wait_send()
            else:
                give_back(group, place).wait_send()


def local(
    residual,
    queries,
    key_rows,
    value_rows,
    diff_scale,
    head_gain,
    out_weight,
    norm_gain,
    gate_weight,
    up_weight,
    down_weight,
    expert_ids,
    route_logit,
):
    sp_size = lax.axis_size("sp")
    tp_size = lax.axis_size("tp")
    tokens, heads, width = value_rows.shape
    feats = residual.shape[1]
    flat = heads * width
    own_block = jnp.stack([key_rows.reshape(tokens, flat), value_rows.reshape(tokens, flat)])
    tops = expert_ids.shape[1]
    cap = -(-(2 * tokens * tops // sp_size) // 16) * 16
    groups = math.gcd(sp_size, 4)
    span = sp_size // groups
    rows = span * cap
    units = gate_weight.shape[2]
    chips = tp_size // 2
    pieces = 8
    early = 6
    dma = pltpu.SemaphoreType.DMA
    vmem = pl.BlockSpec(memory_space=pltpu.VMEM)
    hbm = pl.BlockSpec(memory_space=pl.ANY)
    return pl.pallas_call(
        functools.partial(layer_kernel, sp_size, tp_size, groups, cap, early),
        out_shape=jax.ShapeDtypeStruct((tokens, feats), BF16),
        in_specs=[
            vmem,
            vmem,
            hbm,
            pl.BlockSpec(memory_space=pltpu.SMEM),
            vmem,
            hbm,
            vmem,
            hbm,
            hbm,
            hbm,
            vmem,
            vmem,
        ],
        out_specs=vmem,
        scratch_shapes=[
            pltpu.VMEM((tokens, flat), BF16),
            pltpu.VMEM((sp_size,) + own_block.shape, BF16),
            pltpu.VMEM((heads * 2, tokens, 1), F32),
            pltpu.VMEM((heads * 2, tokens, 1), F32),
            pltpu.VMEM((heads * 2, tokens, width), F32),
            pltpu.VMEM((tp_size, tokens, flat), BF16),
            pltpu.VMEM(out_weight.shape, BF16),
            pltpu.VMEM((tokens, feats), BF16),
            pltpu.VMEM((tokens, tops), jnp.int32),
            pltpu.VMEM((sp_size, cap, feats), BF16),
            pltpu.VMEM((groups, tp_size, rows, feats), BF16),
            pltpu.VMEM((rows, tp_size * feats), BF16),
            pltpu.VMEM((groups, 2, rows, units), BF16),
            pltpu.VMEM((chips, 2 * units, feats), BF16),
            pltpu.VMEM((2, max(rows, tokens), feats), F32),
            pltpu.VMEM((groups, max(chips - 1, 1), rows, feats), BF16),
            pltpu.VMEM((groups, max(chips - 1, 1), rows, feats), BF16),
            pltpu.VMEM((groups, rows, feats), BF16),
            pltpu.VMEM((groups, rows, feats), BF16),
            pltpu.VMEM(gate_weight.shape[1:], BF16),
            pltpu.VMEM(up_weight.shape[1:], BF16),
            dma((4,)),
            dma(()),
            dma((sp_size,)),
            dma((sp_size,)),
            dma((sp_size,)),
            dma((max(chips - 1, 1), pieces)),
            dma((chips, pieces)),
            dma((tp_size,)),
            dma((tp_size,)),
            dma((sp_size,)),
            dma((sp_size,)),
            dma((groups, tp_size)),
            dma((groups, tp_size)),
            dma((groups,)),
            dma((groups,)),
            dma((groups, max(chips - 1, 1))),
            dma((groups, max(chips - 1, 1))),
            dma((sp_size,)),
            dma((sp_size,)),
        ],
        compiler_params=pltpu.CompilerParams(
            collective_id=0, has_side_effects=True, vmem_limit_bytes=56 * 1024 * 1024
        ),
    )(
        residual,
        queries.reshape(tokens, flat),
        own_block,
        diff_scale,
        head_gain[None],
        out_weight,
        norm_gain[None],
        gate_weight[0],
        up_weight[0],
        down_weight[0],
        expert_ids,
        route_logit,
    )


def solution(mesh):
    return jax.shard_map(
        local,
        mesh=mesh,
        in_specs=(
            P("sp", "tp"),
            P("sp", "tp", None),
            P("sp", "tp", None),
            P("sp", "tp", None),
            P("tp"),
            P(),
            P(None, "tp"),
            P(),
            P("sp", None, "tp"),
            P("sp", None, "tp"),
            P("sp", None, "tp"),
            P("sp", None),
            P("sp", None),
        ),
        out_specs=P("sp", "tp"),
        check_vma=False,
    )
```

time: 145 us -> 123 us (0.85)
  the two profiles are of different devices: /device:TPU:0 before, /device:TPU:11 now
where the time goes in v1:
time: 123 us; the launch traced here: 122 us
  Pallas kernels  114 us (93%)
  local copies, waits for them, and re-layouts  8.13 us (7%)
    pallas_call x1, Pallas kernels, local(): pl.pallas_call(functools.partial(layer_kernel, sp_size, tp_size, groups,...  114 us
    unnamed x4, local copies, waits for them, and re-layouts  6.12 us

profile of v1, /device:TPU:11, one launch (start us, length us, event | category | flops | bytes accessed | tf_op | source)
XLA Modules:
  0.0 122.5 jit_solution(5220635159631759376)
XLA Ops:
  0.0 1.0 stack_reshape.6
  1.0 1.0 stack_reshape.7
  2.0 0.8 pad_maximum_fusion.own_block
  2.8 1.6 %copy.18 = bf16[24,8,4,128]{3,1,2,0:T(8,128)(2,1)} copy(bf16[24,8,4,128]{3,2,1,0:T(4,128)(2,1)} %bitcast.13) | data formatting | bytes 393216
  4.4 1.4 %copy.14.expert_ids = s32[192,2]{1,0:T(8,128)} copy(s32[192,2]{0,1:T(2,128)} %param.24) | data formatting | bytes 3072 | tf_op args[11]
  5.9 1.4 %copy.15.route_logit = f32[192,2]{1,0:T(8,128)} copy(f32[192,2]{0,1:T(2,128)} %param.25) | data formatting | bytes 3072 | tf_op args[12]
  7.3 113.6 %shard_map.127 = bf16[192,512]{1,0:T(8,128)(2,1)} custom-call(bf16[192,512]{1,0:T(8,128)(2,1)} %residual.1, bf16[192,512]{1,0:T(8,128)(2,1)} %bitcast.12, bf16[2,192,512]{2,1,0:T(8,128)(2,1)} %pad_maximum_fusion.own_block, f32[4]{0:T(128)} %diff_scale.1, f32[1,128]{1,0:T(1,128)} %bitcast.15, bf16[2048,512]{1,0:T(8,128)(2,1)} %out_hbm.1, f32[1,2048]{1,0:T(1,128)} %bitcast.14, ...), custom_call_target="tpu_custom_call" | custom-call | tf_op jit(solution)/shard_map/pallas_call | solution.py:615
  120.9 1.6 %copy.20 = bf16[192,512]{1,0:T(8,128)(2,1)} copy(bf16[192,512]{1,0:T(8,128)(2,1)} %shard_map.127) | data formatting | bytes 393216

commit v2 on v1

--- a/solution.py
+++ b/solution.py
@@ -29,9 +29,10 @@
     groups,
     cap,
     early,
-    residual,
-    queries,
-    own_block,
+    residual_hbm,
+    query_hbm,
+    key_hbm,
+    value_hbm,
     diff_scale,
     head_gain,
     out_hbm,
@@ -42,10 +43,11 @@
     expert_ids,
     route_logit,
     updated,
+    residual,
+    raw,
     scaled,
     blocks,
     peak,
-    total,
     accum,
     heads_all,
     out_w,
@@ -64,7 +66,7 @@
     gate,
     up,
     weight_sem,
-    block_sem,
+    raw_sem,
     along_send,
     across_send,
     kv_recv,
@@ -91,13 +93,11 @@
     chip = rank // 2
     span = sp_size // groups
     rows = span * cap
-    tokens = queries.shape[0]
-    width = head_gain.shape[1]
-    heads = queries.shape[1] // width
+    tokens, heads, width = query_hbm.shape
     feats = residual.shape[1]
     units = gate.shape[1]
     columns = feats
-    tops = expert_ids.shape[1]
+    tops = expert_ids.shape[0]
 
     def at(index):
         return {"sp": index, "tp": rank}
@@ -118,8 +118,12 @@
             device_id_type=MESH,
         )
 
-    load = pltpu.make_async_copy(own_block, blocks.at[me], block_sem)
-    load.start()
+    raw_loads = [
+        pltpu.make_async_copy(source, raw.at[i], raw_sem.at[i])
+        for i, source in enumerate((key_hbm, value_hbm, query_hbm))
+    ]
+    for copy in raw_loads:
+        copy.start()
     pieces = down_send.shape[1]
     chunk = 2 * units // pieces
     weights = [
@@ -129,9 +133,8 @@
         pltpu.make_async_copy(
             down_hbm.at[pl.ds(chip * 2 * units, 2 * units)], down_part.at[chip], weight_sem.at[3]
         ),
+        pltpu.make_async_copy(residual_hbm, residual, weight_sem.at[4]),
     ]
-    for copy in weights:
-        copy.start()
 
     barrier = pltpu.get_barrier_semaphore()
     for step in range(1, sp_size):
@@ -142,23 +145,34 @@
         pl.semaphore_signal(barrier, inc=1, device_id=beside(peer_rank(step)), device_id_type=MESH)
     pl.semaphore_signal(barrier, inc=1, device_id=beside(sibling), device_id_type=MESH)
 
-    scaled[...] = (queries[...].astype(F32) * QK ** (-0.5)).astype(BF16)
-    total[...] = jnp.zeros(total.shape, F32)
     accum[...] = jnp.zeros(accum.shape, F32)
     peak[...] = jnp.full(peak.shape, NEG_FILL, F32)
 
-    lane = lax.broadcasted_iota(jnp.int32, (tokens, 128), 1)
-    named = [lane == expert_ids[:, k : k + 1] for k in range(tops)]
+    spare = -(-sp_size // 16) * 16
+    names = lax.broadcasted_iota(jnp.int32, (spare, tokens), 0)
+    named = [names == expert_ids[k : k + 1] for k in range(tops)]
     both = functools.reduce(jnp.logical_or, named).astype(F32).astype(BF16)
     before = (
-        lax.broadcasted_iota(jnp.int32, (tokens, tokens), 1)
-        < lax.broadcasted_iota(jnp.int32, (tokens, tokens), 0)
+        lax.broadcasted_iota(jnp.int32, (tokens, tokens), 0)
+        < lax.broadcasted_iota(jnp.int32, (tokens, tokens), 1)
     ).astype(F32).astype(BF16)
-    earlier = jnp.dot(before, both, preferred_element_type=F32)
+    earlier = jnp.dot(both, before, preferred_element_type=F32)
+    peak_logit = jnp.max(route_logit[...], axis=0, keepdims=True)
+    shares = jnp.exp(route_logit[...] - peak_logit)
+    shares = shares / jnp.sum(shares, axis=0, keepdims=True)
     for k in range(tops):
-        order = jnp.sum(jnp.where(named[k], earlier, 0.0), axis=1, keepdims=True)
-        step_of = lax.rem(me + sp_size - expert_ids[:, k : k + 1], sp_size)
-        places[:, k : k + 1] = step_of * cap + order.astype(jnp.int32)
+        order = jnp.sum(jnp.where(named[k], earlier, 0.0), axis=0, keepdims=True)
+        step_of = lax.rem(me + sp_size - expert_ids[k : k + 1], sp_size)
+        places[k : k + 1] = step_of * cap + order.astype(jnp.int32)
+
+    for i in range(2):
+        raw_loads[i].wait()
+        blocks[me, i] = jnp.transpose(raw[i], (1, 0, 2))
+    raw_loads[2].wait()
+    low = lax.broadcasted_iota(jnp.int32, (heads, tokens, width), 2) < QK
+    query = jnp.transpose(raw[2], (1, 0, 2)).astype(F32) * QK ** (-0.5)
+    scaled[0] = jnp.where(low, query, 0.0).astype(BF16)
+    scaled[1] = jnp.where(low, 0.0, query).astype(BF16)
 
     pl.semaphore_wait(barrier, sp_size - 1 + chips)
 
@@ -178,8 +192,6 @@
             def _(piece):
                 down_piece(step, piece).start()
 
-    load.wait()
-
     pairs = sp_size // 2
     pair = me // 2
     side = lax.rem(me, 2)
@@ -192,16 +204,17 @@
 
     def attend(block, masked):
         if masked:
-            row = me * tokens + lax.broadcasted_iota(jnp.int32, (tokens, tokens), 0)
-            col = block * tokens + lax.broadcasted_iota(jnp.int32, (tokens, tokens), 1)
-            visible = col // SPAN <= row // SPAN
+            key = block * tokens + lax.broadcasted_iota(jnp.int32, (tokens, tokens), 0)
+            query = me * tokens + lax.broadcasted_iota(jnp.int32, (tokens, tokens), 1)
+            visible = key // SPAN <= query // SPAN
         for head in range(heads):
-            value = blocks[block, 1, :, head * width : (head + 1) * width]
+            value = jnp.concatenate(
+                [jnp.transpose(blocks[block, 1, head]), jnp.ones((16, tokens), BF16)], axis=0
+            )
             for half in range(2):
-                start = head * width + half * QK
                 scores = lax.dot_general(
-                    scaled[:, start : start + QK],
-                    blocks[block, 0, :, start : start + QK],
+                    blocks[block, 0, head],
+                    scaled[half, head],
                     (((1,), (1,)), ((), ())),
                     preferred_element_type=F32,
                 )
@@ -209,15 +222,13 @@
                     scores = jnp.where(visible, scores, NEG_FILL)
                 index = head * 2 + half
                 old = peak[index]
-                new = jnp.maximum(old, jnp.max(scores, axis=-1, keepdims=True))
+                new = jnp.maximum(old, jnp.max(scores, axis=0, keepdims=True))
                 exps = jnp.exp(scores - new)
                 if masked:
                     exps = jnp.where(visible, exps, 0.0)
-                rescale = jnp.exp(old - new)
                 peak[index] = new
-                total[index] = total[index] * rescale + jnp.sum(exps, axis=-1, keepdims=True)
-                accum[index] = accum[index] * rescale + jnp.dot(
-                    exps.astype(BF16), value, preferred_element_type=F32
+                accum[index] = accum[index] * jnp.exp(old - new) + jnp.dot(
+                    value, exps.astype(BF16), preferred_element_type=F32
                 )
 
     plain_blocks = tokens % SPAN == 0
@@ -243,6 +254,8 @@
         @pl.when(back == 0)
         def _():
             send_down(0, early)
+            for copy in weights:
+                copy.start()
             attend(me, True)
 
         second = other - 2 * (back - 1)
@@ -294,44 +307,56 @@
         piece(buffer, send, recv, rank, sibling, sibling).wait_send()
 
     for head in range(heads):
-        first = accum[head * 2] / total[head * 2]
-        later = accum[head * 2 + 1] / total[head * 2 + 1]
-        mixture = first - diff_scale[head] * later
-        scale_back = lax.rsqrt(jnp.mean(mixture * mixture, axis=-1, keepdims=True) + NORM_EPS)
-        heads_all[rank, :, head * width : (head + 1) * width] = (
-            mixture * scale_back * head_gain[...] * HEAD_KEEP
+        maps = [
+            accum[index, :width] / accum[index, width : width + 1]
+            for index in (head * 2, head * 2 + 1)
+        ]
+        mixture = maps[0] - diff_scale[head] * maps[1]
+        scale_back = lax.rsqrt(jnp.mean(mixture * mixture, axis=0, keepdims=True) + NORM_EPS)
+        heads_all[head, rank] = (
+            jnp.transpose(mixture * scale_back) * head_gain[...] * HEAD_KEEP
         ).astype(BF16)
-    spread(heads_all, att_send, att_recv)
+        spread(heads_all.at[head], att_send.at[head], att_recv.at[head])
     send_down(early, pieces)
     weights[0].wait()
+    weights[4].wait()
 
     def project(owner):
         return jnp.dot(
-            heads_all[owner],
+            jnp.concatenate([heads_all[head, owner] for head in range(heads)], axis=1),
             out_w[pl.ds(pl.multiple_of(owner * heads * width, heads * width), heads * width)],
             preferred_element_type=F32,
         )
 
     sums = own_sum.at[0, pl.ds(0, tokens)]
     sums[...] = residual[...].astype(F32) + project(rank)
-    collect(heads_all, att_send, att_recv)
-    for step in range(chips):
+    for head in range(heads):
+        for step in range(1, chips):
+            forward(heads_all.at[head], att_send.at[head], att_recv.at[head], step)
+
+    def from_sibling(step):
         owner = peer_rank(step) + 1 - 2 * parity
-        sums[...] += project(owner)
-        if step > 0:
-            sums[...] += project(peer_rank(step))
+        for head in range(heads):
+            piece(
+                heads_all.at[head], att_send.at[head], att_recv.at[head], owner, sibling, sibling
+            ).wait_recv()
+        return project(owner)
+
+    sums[...] += from_sibling(0)
+    for step in range(1, chips):
+        sums[...] += project(peer_rank(step))
+    for step in range(1, chips):
+        sums[...] += from_sibling(step)
     mixer[...] = sums[...].astype(BF16)
 
     def slots_of(first, count):
-        slot = first + lax.broadcasted_iota(jnp.int32, (tokens, count), 1)
-        return [
-            (slot == places[:, k : k + 1]).astype(F32).astype(BF16) for k in range(tops)
-        ]
+        slot = first + lax.broadcasted_iota(jnp.int32, (count, tokens), 0)
+        return [slot == places[k : k + 1] for k in range(tops)]
 
     def chosen_rows(step):
-        held = functools.reduce(jnp.add, slots_of(step * cap, cap))
-        return lax.dot_general(
-            held, mixer[...], (((0,), (0,)), ((), ())), preferred_element_type=F32
+        held = functools.reduce(jnp.logical_or, slots_of(step * cap, cap))
+        return jnp.dot(
+            held.astype(F32).astype(BF16), mixer[...], preferred_element_type=F32
         ).astype(BF16)
 
     def dispatch(step):
@@ -518,9 +543,6 @@
         def _():
             run_down(turn - 2)
 
-    peak_logit = jnp.max(route_logit[...], axis=-1, keepdims=True)
-    shares = jnp.exp(route_logit[...] - peak_logit)
-    shares = shares / jnp.sum(shares, axis=-1, keepdims=True)
     back_sum = own_sum.at[0, pl.ds(0, tokens)]
     back_sum[...] = mixer[...].astype(F32)
 
@@ -533,10 +555,16 @@
                     give_back(group, 0).wait_recv()
             else:
                 give_back(group, place).wait_recv()
+        portion = 0.0
+        for k, held in enumerate(slots_of(group * rows, rows)):
+            portion += jnp.where(held, shares[k : k + 1], 0.0)
+        coarse = portion.astype(BF16)
+        fine = (portion - coarse.astype(F32)).astype(BF16)
         routed = 0.0
-        for k, held in enumerate(slots_of(group * rows, rows)):
-            picked = jnp.dot(held, returned[group], preferred_element_type=F32)
-            routed += picked * shares[:, k : k + 1]
+        for part in (coarse, fine):
+            routed += lax.dot_general(
+                part, returned[group], (((0,), (0,)), ((), ())), preferred_element_type=F32
+            )
         back_sum[...] += routed
 
     updated[...] = back_sum[...].astype(BF16)
@@ -558,7 +586,8 @@
         def _(index):
             down_piece(step, index).wait_send()
 
-    settle(heads_all, att_send, att_recv)
+    for head in range(heads):
+        settle(heads_all.at[head], att_send.at[head], att_recv.at[head])
 
     @pl.loop(1, sp_size)
     def _(step):
@@ -598,8 +627,6 @@
     tp_size = lax.axis_size("tp")
     tokens, heads, width = value_rows.shape
     feats = residual.shape[1]
-    flat = heads * width
-    own_block = jnp.stack([key_rows.reshape(tokens, flat), value_rows.reshape(tokens, flat)])
     tops = expert_ids.shape[1]
     cap = -(-(2 * tokens * tops // sp_size) // 16) * 16
     groups = math.gcd(sp_size, 4)
@@ -607,8 +634,8 @@
     rows = span * cap
     units = gate_weight.shape[2]
     chips = tp_size // 2
-    pieces = 8
-    early = 6
+    pieces = 16
+    early = 13
     dma = pltpu.SemaphoreType.DMA
     vmem = pl.BlockSpec(memory_space=pltpu.VMEM)
     hbm = pl.BlockSpec(memory_space=pl.ANY)
@@ -616,8 +643,9 @@
         functools.partial(layer_kernel, sp_size, tp_size, groups, cap, early),
         out_shape=jax.ShapeDtypeStruct((tokens, feats), BF16),
         in_specs=[
-            vmem,
-            vmem,
+            hbm,
+            hbm,
+            hbm,
             hbm,
             pl.BlockSpec(memory_space=pltpu.SMEM),
             vmem,
@@ -631,15 +659,16 @@
         ],
         out_specs=vmem,
         scratch_shapes=[
-            pltpu.VMEM((tokens, flat), BF16),
-            pltpu.VMEM((sp_size,) + own_block.shape, BF16),
-            pltpu.VMEM((heads * 2, tokens, 1), F32),
-            pltpu.VMEM((heads * 2, tokens, 1), F32),
-            pltpu.VMEM((heads * 2, tokens, width), F32),
-            pltpu.VMEM((tp_size, tokens, flat), BF16),
+            pltpu.VMEM((tokens, feats), BF16),
+            pltpu.VMEM((3, tokens, heads, width), BF16),
+            pltpu.VMEM((2, heads, tokens, width), BF16),
+            pltpu.VMEM((sp_size, 2, heads, tokens, width), BF16),
+            pltpu.VMEM((heads * 2, 1, tokens), F32),
+            pltpu.VMEM((heads * 2, width + 16, tokens), F32),
+            pltpu.VMEM((heads, tp_size, tokens, width), BF16),
             pltpu.VMEM(out_weight.shape, BF16),
             pltpu.VMEM((tokens, feats), BF16),
-            pltpu.VMEM((tokens, tops), jnp.int32),
+            pltpu.VMEM((tops, tokens), jnp.int32),
             pltpu.VMEM((sp_size, cap, feats), BF16),
             pltpu.VMEM((groups, tp_size, rows, feats), BF16),
             pltpu.VMEM((rows, tp_size * feats), BF16),
@@ -652,15 +681,15 @@
             pltpu.VMEM((groups, rows, feats), BF16),
             pltpu.VMEM(gate_weight.shape[1:], BF16),
             pltpu.VMEM(up_weight.shape[1:], BF16),
-            dma((4,)),
-            dma(()),
+            dma((5,)),
+            dma((3,)),
             dma((sp_size,)),
             dma((sp_size,)),
             dma((sp_size,)),
             dma((max(chips - 1, 1), pieces)),
             dma((chips, pieces)),
-            dma((tp_size,)),
-            dma((tp_size,)),
+            dma((heads, tp_size)),
+            dma((heads, tp_size)),
             dma((sp_size,)),
             dma((sp_size,)),
             dma((groups, tp_size)),
@@ -677,8 +706,9 @@
         ),
     )(
         residual,
-        queries.reshape(tokens, flat),
-        own_block,
+        queries,
+        key_rows,
+        value_rows,
         diff_scale,
         head_gain[None],
         out_weight,
@@ -686,8 +716,8 @@
         gate_weight[0],
         up_weight[0],
         down_weight[0],
-        expert_ids,
-        route_logit,
+        expert_ids.T,
+        route_logit.T,
     )
 
 

time: 123 us -> 117 us (0.951)
  the two profiles are of different devices: /device:TPU:11 before, /device:TPU:0 now
where the time goes in v2:
time: 117 us
  Pallas kernels  115 us (98%)
  local copies, waits for them, and re-layouts  1.62 us (1%)
    pallas_call x1, Pallas kernels, local(): pl.pallas_call(functools.partial(layer_kernel, sp_size, tp_size, groups,...  115 us

profile of v2, /device:TPU:0, one launch (start us, length us, event | category | flops | bytes accessed | tf_op | source)
XLA Modules:
  0.0 116.7 jit_solution(10049843277657357969)
XLA Ops:
  0.0 115.0 %shard_map.127 = bf16[192,512]{1,0:T(8,128)(2,1)} custom-call(bf16[192,512]{1,0:T(8,128)(2,1)} %residual_hbm.1, bf16[192,4,128]{2,1,0:T(4,128)(2,1)} %query_hbm.1, bf16[192,4,128]{2,1,0:T(4,128)(2,1)} %key_hbm.1, bf16[192,4,128]{2,1,0:T(4,128)(2,1)} %value_hbm.1, f32[4]{0:T(128)} %diff_scale.1, f32[1,128]{1,0:T(1,128)} %bitcast.13, ...), custom_call_target="tpu_custom_call" | custom-call | tf_op jit(solution)/shard_map/pallas_call | solution.py:642
  115.0 1.6 %copy.15 = bf16[192,512]{1,0:T(8,128)(2,1)} copy(bf16[192,512]{1,0:T(8,128)(2,1)} %shard_map.127) | data formatting | bytes 393216

commit v3 on v2

--- a/solution.py
+++ b/solution.py
@@ -53,16 +53,24 @@
     out_w,
     mixer,
     places,
-    outgoing,
-    rows_in,
+    near_out,
+    far_out,
+    near_rows,
+    far_rows,
     normed,
-    hidden,
+    near_hidden,
+    far_hidden,
     down_part,
     own_sum,
+    far_sum,
     part_send,
     part_recv,
-    result,
-    returned,
+    near_result,
+    far_result,
+    near_back,
+    far_back,
+    share_send,
+    share_recv,
     gate,
     up,
     weight_sem,
@@ -74,16 +82,26 @@
     down_recv,
     att_send,
     att_recv,
-    disp_send,
-    disp_recv,
+    mix_send,
+    mix_recv,
+    near_send,
+    near_recv,
+    far_send,
+    far_recv,
+    pair_send,
+    pair_recv,
     row_send,
     row_recv,
     hid_send,
     hid_recv,
     sum_send,
     sum_recv,
-    ret_send,
-    ret_recv,
+    near_ret_send,
+    near_ret_recv,
+    far_ret_send,
+    far_ret_recv,
+    share_send_sem,
+    share_recv_sem,
 ):
     me = lax.axis_index("sp")
     rank = lax.axis_index("tp")
@@ -91,8 +109,12 @@
     sibling = rank + 1 - 2 * parity
     chips = tp_size // 2
     chip = rank // 2
-    span = sp_size // groups
+    reach = sp_size // 2
+    half_of = me // reach
+    spot = lax.rem(me, reach)
+    span = reach // groups
     rows = span * cap
+    near_count = reach * cap
     tokens, heads, width = query_hbm.shape
     feats = residual.shape[1]
     units = gate.shape[1]
@@ -162,7 +184,9 @@
     shares = shares / jnp.sum(shares, axis=0, keepdims=True)
     for k in range(tops):
         order = jnp.sum(jnp.where(named[k], earlier, 0.0), axis=0, keepdims=True)
-        step_of = lax.rem(me + sp_size - expert_ids[k : k + 1], sp_size)
+        expert = expert_ids[k : k + 1]
+        apart = jnp.where(expert // reach == half_of, 0, reach)
+        step_of = lax.rem(spot + reach - lax.rem(expert, reach), reach) + apart
         places[k : k + 1] = step_of * cap + order.astype(jnp.int32)
 
     for i in range(2):
@@ -328,7 +352,7 @@
             preferred_element_type=F32,
         )
 
-    sums = own_sum.at[0, pl.ds(0, tokens)]
+    sums = own_sum
     sums[...] = residual[...].astype(F32) + project(rank)
     for head in range(heads):
         for step in range(1, chips):
@@ -347,95 +371,170 @@
         sums[...] += project(peer_rank(step))
     for step in range(1, chips):
         sums[...] += from_sibling(step)
-    mixer[...] = sums[...].astype(BF16)
+    mixer[chip] = sums[...].astype(BF16)
+
+    def mix_copy(step):
+        target = lax.rem(chip + step, chips)
+        return remote(
+            mixer.at[chip],
+            mixer.at[chip],
+            mix_send.at[step - 1],
+            mix_recv.at[chip],
+            beside(target * 2 + parity),
+        )
+
+    for step in range(1, chips):
+        mix_copy(step).start()
 
     def slots_of(first, count):
         slot = first + lax.broadcasted_iota(jnp.int32, (count, tokens), 0)
         return [slot == places[k : k + 1] for k in range(tops)]
 
-    def chosen_rows(step):
+    def chosen_rows(step, source):
         held = functools.reduce(jnp.logical_or, slots_of(step * cap, cap))
         return jnp.dot(
-            held.astype(F32).astype(BF16), mixer[...], preferred_element_type=F32
+            held.astype(F32).astype(BF16), mixer[source], preferred_element_type=F32
         ).astype(BF16)
 
-    def dispatch(step):
-        expert = lax.rem(me + sp_size - step, sp_size)
-        return remote(
-            outgoing.at[step],
-            rows_in.at[step // span, rank, pl.ds(lax.rem(step, span) * cap, cap)],
-            disp_send.at[step],
-            disp_recv.at[step],
-            at(expert),
-        )
-
-    rows_in[0, rank, pl.ds(0, cap), :] = chosen_rows(0)
-
-    @pl.loop(1, sp_size)
-    def _(step):
-        outgoing[step] = chosen_rows(step)
-        dispatch(step).start()
+    def near_at(place):
+        return at(half_of * reach + lax.rem(spot + reach + place, reach))
+
+    def far_at(place):
+        return at((1 - half_of) * reach + lax.rem(spot + reach + place, reach))
+
+    def far_dispatch(place):
+        return remote(
+            far_out.at[place],
+            far_rows.at[place // span, rank, pl.ds(lax.rem(place, span) * cap, cap)],
+            far_send.at[place],
+            far_recv.at[place],
+            far_at(-place),
+        )
+
+    def near_dispatch(place, source):
+        return remote(
+            near_out.at[place, source],
+            near_rows.at[source * 2 + parity, pl.ds(place * cap, cap)],
+            near_send.at[place, source],
+            near_recv.at[place, source],
+            near_at(-place),
+        )
+
+    def send_near(source):
+        near_rows[source * 2 + parity, pl.ds(0, cap), :] = chosen_rows(0, source)
+
+        @pl.loop(1, reach)
+        def _(place):
+            near_out[place, source] = chosen_rows(place, source)
+            near_dispatch(place, source).start()
+
+    @pl.loop(0, reach)
+    def _(place):
+        far_out[place] = chosen_rows(reach + place, chip)
+        far_dispatch(place).start()
+
+    send_near(chip)
+    for step in range(1, chips):
+        source = lax.rem(chip + step, chips)
+        remote(
+            mixer.at[source],
+            mixer.at[source],
+            mix_send.at[step - 1],
+            mix_recv.at[source],
+            beside(sibling),
+        ).wait_recv()
+        send_near(source)
 
     unit_tile = math.gcd(units, 256)
     column_tile = math.gcd(columns, 256)
 
     def spread_rows(group):
         for place in range(span):
-            step = group * span + place
-            arrived = remote(
-                outgoing.at[0],
-                rows_in.at[group, rank, pl.ds(place * cap, cap)],
-                disp_send.at[step],
-                disp_recv.at[step],
+            remote(
+                far_out.at[0],
+                far_rows.at[group, rank, pl.ds(place * cap, cap)],
+                far_send.at[group * span + place],
+                far_recv.at[group * span + place],
                 beside(sibling),
-            )
-            if place == 0:
-                @pl.when(group > 0)
-                def _():
-                    arrived.wait_recv()
-            else:
-                arrived.wait_recv()
-        spread(rows_in.at[group], row_send.at[group], row_recv.at[group])
-
-    def hidden_copy(group):
-        return remote(
-            hidden.at[group, parity],
-            hidden.at[group, parity],
-            hid_send.at[group],
-            hid_recv.at[group],
+            ).wait_recv()
+        spread(far_rows.at[group], row_send.at[group], row_recv.at[group])
+
+    def pair_copy(source):
+        return remote(
+            near_rows.at[source * 2 + parity],
+            near_rows.at[source * 2 + parity],
+            pair_send.at[source],
+            pair_recv.at[source],
             beside(sibling),
         )
 
-    def run_up(group):
-        collect(rows_in.at[group], row_send.at[group], row_recv.at[group])
-
-        @pl.when(group == 0)
-        def _():
-            weights[1].wait()
-            weights[2].wait()
-
+    def pair_rows():
+        for step in range(chips):
+            source = lax.rem(chip + step, chips)
+
+            @pl.loop(1, reach)
+            def _(place):
+                remote(
+                    near_out.at[0, 0],
+                    near_rows.at[source * 2 + parity, pl.ds(place * cap, cap)],
+                    near_send.at[place, source],
+                    near_recv.at[place, source],
+                    beside(sibling),
+                ).wait_recv()
+
+            pair_copy(source).start()
+
+    def pair_wait():
+        for step in range(chips):
+            source = lax.rem(chip + step, chips)
+            remote(
+                near_rows.at[source * 2 + 1 - parity],
+                near_rows.at[source * 2 + 1 - parity],
+                pair_send.at[source],
+                pair_recv.at[source],
+                beside(sibling),
+            ).wait_recv()
+
+    def hidden_copy(hidden, index, core):
+        return remote(
+            hidden.at[core],
+            hidden.at[core],
+            hid_send.at[index],
+            hid_recv.at[index],
+            beside(sibling),
+        )
+
+    def run_up(table, hidden, count, index):
         square = 0.0
         for part in range(tp_size):
-            value = rows_in[group, part].astype(F32)
+            value = table[part].astype(F32)
             square += jnp.sum(value * value, axis=-1, keepdims=True)
         scale_back = lax.rsqrt(square / (tp_size * feats) + NORM_EPS)
         for part in range(tp_size):
             depth = slice(part * feats, (part + 1) * feats)
-            normed[:, depth] = (
-                rows_in[group, part].astype(F32) * scale_back * norm_gain[:, depth]
+            normed[:count, depth] = (
+                table[part].astype(F32) * scale_back * norm_gain[:, depth]
             ).astype(BF16)
 
         @pl.loop(0, units // unit_tile)
         def _(tile):
             cols = pl.ds(pl.multiple_of(tile * unit_tile, unit_tile), unit_tile)
-            pre_gate = jnp.dot(normed[...], gate[:, cols], preferred_element_type=F32)
-            pre_up = jnp.dot(normed[...], up[:, cols], preferred_element_type=F32)
+            pre_gate = jnp.dot(normed[:count], gate[:, cols], preferred_element_type=F32)
+            pre_up = jnp.dot(normed[:count], up[:, cols], preferred_element_type=F32)
             capped = jnp.minimum(pre_gate, CLAMP_LIMIT)
             linear = jnp.clip(pre_up, -CLAMP_LIMIT, CLAMP_LIMIT)
             value = capped * jax.nn.sigmoid(SWISH_ALPHA * capped) * (linear + 1.0)
-            hidden[group, parity, :, cols] = value.astype(BF16)
-
-        hidden_copy(group).start()
+            hidden[parity, :, cols] = value.astype(BF16)
+
+        hidden_copy(hidden, index, parity).start()
+
+    def far_up(group):
+        collect(far_rows.at[group], row_send.at[group], row_recv.at[group])
+        run_up(far_rows.at[group], far_hidden.at[group], rows, group)
+
+    def near_up():
+        pair_wait()
+        run_up(near_rows, near_hidden, near_count, groups)
 
     def sum_copy(group, step):
         target = lax.rem(chip + step, chips)
@@ -447,127 +546,173 @@
             beside(target * 2 + parity),
         )
 
-    def part_sum(group, block, cols):
+    def part_sum(hidden, block, cols):
         value = 0.0
         for core in range(2):
             value += jnp.dot(
-                hidden[group, core],
+                hidden[core],
                 down_part[block, core * units : (core + 1) * units, cols],
                 preferred_element_type=F32,
             )
         return value
 
-    def run_down(group):
-        remote(
-            hidden.at[group, 1 - parity],
-            hidden.at[group, 1 - parity],
-            hid_send.at[group],
-            hid_recv.at[group],
-            beside(sibling),
-        ).wait_recv()
-
-        @pl.when(group == 0)
-        def _():
-            weights[3].wait()
-            for step in range(1, chips):
-                source = lax.rem(chip + step, chips)
-
-                @pl.loop(0, pieces)
-                def _(index):
-                    remote(
-                        down_part.at[source, pl.ds(index * chunk, chunk)],
-                        down_part.at[source, pl.ds(index * chunk, chunk)],
-                        down_send.at[step - 1, index],
-                        down_recv.at[source, index],
-                        beside(sibling),
-                    ).wait_recv()
-
-        for step in range(1, chips):
-            @pl.loop(0, columns // column_tile)
-            def _(tile):
-                cols = pl.ds(pl.multiple_of(tile * column_tile, column_tile), column_tile)
-                part_send[group, step - 1, :, cols] = part_sum(
-                    group, lax.rem(chip + step, chips), cols
-                ).astype(BF16)
-
-            sum_copy(group, step).start()
-
+    def column_loop(body):
         @pl.loop(0, columns // column_tile)
         def _(tile):
-            cols = pl.ds(pl.multiple_of(tile * column_tile, column_tile), column_tile)
-            own_sum[lax.rem(group, 2), pl.ds(0, rows), cols] = part_sum(group, chip, cols)
-
-    def give_back(group, place):
-        step = group * span + place
-        return remote(
-            result.at[group, pl.ds(place * cap, cap)],
-            returned.at[group, pl.ds(place * cap, cap)],
-            ret_send.at[step],
-            ret_recv.at[step],
-            at(lax.rem(me + step, sp_size)),
+            body(pl.ds(pl.multiple_of(tile * column_tile, column_tile), column_tile))
+
+    def down_ready():
+        weights[3].wait()
+        for step in range(1, chips):
+            source = lax.rem(chip + step, chips)
+
+            @pl.loop(0, pieces)
+            def _(index):
+                remote(
+                    down_part.at[source, pl.ds(index * chunk, chunk)],
+                    down_part.at[source, pl.ds(index * chunk, chunk)],
+                    down_send.at[step - 1, index],
+                    down_recv.at[source, index],
+                    beside(sibling),
+                ).wait_recv()
+
+    def far_down(group):
+        hidden_copy(far_hidden.at[group], group, 1 - parity).wait_recv()
+        for step in range(1, chips):
+            def outward(cols):
+                part_send[group, step - 1, :, cols] = part_sum(
+                    far_hidden.at[group], lax.rem(chip + step, chips), cols
+                ).astype(BF16)
+
+            column_loop(outward)
+            sum_copy(group, step).start()
+
+        def inward(cols):
+            far_sum[group, :, cols] = part_sum(far_hidden.at[group], chip, cols)
+
+        column_loop(inward)
+
+    def near_return(place, block):
+        return remote(
+            near_result.at[block, pl.ds(place * cap, cap)],
+            near_back.at[block, pl.ds(place * cap, cap)],
+            near_ret_send.at[place, block],
+            near_ret_recv.at[place, block],
+            near_at(place),
+        )
+
+    def near_down():
+        hidden_copy(near_hidden, groups, 1 - parity).wait_recv()
+        for step in range(1, chips + 1):
+            block = lax.rem(chip + step, chips)
+
+            def store(cols):
+                near_result[block, :, cols] = part_sum(near_hidden, block, cols).astype(BF16)
+
+            column_loop(store)
+
+            @pl.loop(1, reach)
+            def _(place):
+                near_return(place, block).start()
+
+            near_back[block, pl.ds(0, cap), :] = near_result[block, pl.ds(0, cap), :]
+
+    def give_back(place):
+        return remote(
+            far_result.at[place // span, pl.ds(lax.rem(place, span) * cap, cap)],
+            far_back.at[place // span, pl.ds(lax.rem(place, span) * cap, cap)],
+            far_ret_send.at[place],
+            far_ret_recv.at[place],
+            far_at(place),
         )
 
     def finish(group):
-        value = own_sum[lax.rem(group, 2), pl.ds(0, rows), :]
+        value = far_sum[group]
         for step in range(1, chips):
             sum_copy(group, step).wait_recv()
             value += part_recv[group, step - 1].astype(F32)
-        result[group] = value.astype(BF16)
+        far_result[group] = value.astype(BF16)
         for place in range(span):
-            if place == 0:
-                @pl.when(group == 0)
-                def _():
-                    returned[0, pl.ds(0, cap), :] = result[0, pl.ds(0, cap), :]
-
-                @pl.when(group > 0)
-                def _():
-                    give_back(group, 0).start()
-            else:
-                give_back(group, place).start()
-
-    @pl.loop(0, groups + 3)
+            give_back(group * span + place).start()
+
+    spread_rows(0)
+    pair_rows()
+    weights[1].wait()
+    weights[2].wait()
+    near_up()
+
+    @pl.loop(0, groups + 2)
     def _(turn):
+        @pl.when(turn < groups - 1)
+        def _():
+            spread_rows(turn + 1)
+
         @pl.when(turn < groups)
         def _():
-            spread_rows(turn)
+            far_up(turn)
+
+        @pl.when(turn == 1)
+        def _():
+            down_ready()
+
+        @pl.when(turn >= 2)
+        def _():
+            finish(turn - 2)
 
         @pl.when((turn >= 1) & (turn < groups + 1))
         def _():
-            run_up(turn - 1)
-
-        @pl.when((turn >= 3))
+            far_down(turn - 1)
+
+        @pl.when(turn == 1)
         def _():
-            finish(turn - 3)
-
-        @pl.when((turn >= 2) & (turn < groups + 2))
-        def _():
-            run_down(turn - 2)
-
-    back_sum = own_sum.at[0, pl.ds(0, tokens)]
-    back_sum[...] = mixer[...].astype(F32)
+            near_down()
+
+    def routed_sum(first, count, table):
+        portion = 0.0
+        for k, held in enumerate(slots_of(first, count)):
+            portion += jnp.where(held, shares[k : k + 1], 0.0)
+        coarse = portion.astype(BF16)
+        fine = (portion - coarse.astype(F32)).astype(BF16)
+        value = 0.0
+        for part in (coarse, fine):
+            value += lax.dot_general(
+                part, table, (((0,), (0,)), ((), ())), preferred_element_type=F32
+            )
+        return value
+
+    def share_copy(step):
+        target = lax.rem(chip + step, chips)
+        return remote(
+            share_send.at[step - 1],
+            share_recv.at[step - 1],
+            share_send_sem.at[step - 1],
+            share_recv_sem.at[step - 1],
+            beside(target * 2 + parity),
+        )
+
+    for step in range(1, chips + 1):
+        block = lax.rem(chip + step, chips)
+
+        @pl.loop(1, reach)
+        def _(place):
+            near_return(place, block).wait_recv()
+
+        if step < chips:
+            share_send[step - 1] = routed_sum(0, near_count, near_back[block]).astype(BF16)
+            share_copy(step).start()
+        else:
+            sums[...] = mixer[chip].astype(F32) + routed_sum(0, near_count, near_back[chip])
 
     @pl.loop(0, groups)
     def _(group):
         for place in range(span):
-            if place == 0:
-                @pl.when(group > 0)
-                def _():
-                    give_back(group, 0).wait_recv()
-            else:
-                give_back(group, place).wait_recv()
-        portion = 0.0
-        for k, held in enumerate(slots_of(group * rows, rows)):
-            portion += jnp.where(held, shares[k : k + 1], 0.0)
-        coarse = portion.astype(BF16)
-        fine = (portion - coarse.astype(F32)).astype(BF16)
-        routed = 0.0
-        for part in (coarse, fine):
-            routed += lax.dot_general(
-                part, returned[group], (((0,), (0,)), ((), ())), preferred_element_type=F32
-            )
-        back_sum[...] += routed
-
-    updated[...] = back_sum[...].astype(BF16)
+            give_back(group * span + place).wait_recv()
+        sums[...] += routed_sum(near_count + group * rows, rows, far_back[group])
+
+    for step in range(1, chips):
+        share_copy(step).wait_recv()
+        sums[...] += share_recv[step - 1].astype(F32)
+    updated[...] = sums[...].astype(BF16)
 
     @pl.loop(0, pair + 1)
     def _(back):
@@ -589,23 +734,31 @@
     for head in range(heads):
         settle(heads_all.at[head], att_send.at[head], att_recv.at[head])
 
-    @pl.loop(1, sp_size)
-    def _(step):
-        dispatch(step).wait_send()
+    for step in range(1, chips):
+        mix_copy(step).wait_send()
+        share_copy(step).wait_send()
+
+    @pl.loop(0, reach)
+    def _(place):
+        far_dispatch(place).wait_send()
+        give_back(place).wait_send()
+
+    for source in range(chips):
+        pair_copy(source).wait_send()
+
+        @pl.loop(1, reach)
+        def _(place):
+            near_dispatch(place, source).wait_send()
+            near_return(place, source).wait_send()
+
+    hidden_copy(near_hidden, groups, parity).wait_send()
 
     @pl.loop(0, groups)
     def _(group):
-        settle(rows_in.at[group], row_send.at[group], row_recv.at[group])
-        hidden_copy(group).wait_send()
+        settle(far_rows.at[group], row_send.at[group], row_recv.at[group])
+        hidden_copy(far_hidden.at[group], group, parity).wait_send()
         for step in range(1, chips):
             sum_copy(group, step).wait_send()
-        for place in range(span):
-            if place == 0:
-                @pl.when(group > 0)
-                def _():
-                    give_back(group, 0).wait_send()
-            else:
-                give_back(group, place).wait_send()
 
 
 def local(
@@ -629,11 +782,13 @@
     feats = residual.shape[1]
     tops = expert_ids.shape[1]
     cap = -(-(2 * tokens * tops // sp_size) // 16) * 16
-    groups = math.gcd(sp_size, 4)
-    span = sp_size // groups
-    rows = span * cap
+    reach = sp_size // 2
+    groups = math.gcd(reach, 4)
+    rows = reach // groups * cap
+    near_count = reach * cap
     units = gate_weight.shape[2]
     chips = tp_size // 2
+    peers = max(chips - 1, 1)
     pieces = 16
     early = 13
     dma = pltpu.SemaphoreType.DMA
@@ -667,18 +822,26 @@
             pltpu.VMEM((heads * 2, width + 16, tokens), F32),
             pltpu.VMEM((heads, tp_size, tokens, width), BF16),
             pltpu.VMEM(out_weight.shape, BF16),
-            pltpu.VMEM((tokens, feats), BF16),
+            pltpu.VMEM((chips, tokens, feats), BF16),
             pltpu.VMEM((tops, tokens), jnp.int32),
-            pltpu.VMEM((sp_size, cap, feats), BF16),
+            pltpu.VMEM((reach, chips, cap, feats), BF16),
+            pltpu.VMEM((reach, cap, feats), BF16),
+            pltpu.VMEM((tp_size, near_count, feats), BF16),
             pltpu.VMEM((groups, tp_size, rows, feats), BF16),
-            pltpu.VMEM((rows, tp_size * feats), BF16),
+            pltpu.VMEM((near_count, tp_size * feats), BF16),
+            pltpu.VMEM((2, near_count, units), BF16),
             pltpu.VMEM((groups, 2, rows, units), BF16),
             pltpu.VMEM((chips, 2 * units, feats), BF16),
-            pltpu.VMEM((2, max(rows, tokens), feats), F32),
-            pltpu.VMEM((groups, max(chips - 1, 1), rows, feats), BF16),
-            pltpu.VMEM((groups, max(chips - 1, 1), rows, feats), BF16),
+            pltpu.VMEM((tokens, feats), F32),
+            pltpu.VMEM((groups, rows, feats), F32),
+            pltpu.VMEM((groups, peers, rows, feats), BF16),
+            pltpu.VMEM((groups, peers, rows, feats), BF16),
+            pltpu.VMEM((chips, near_count, feats), BF16),
             pltpu.VMEM((groups, rows, feats), BF16),
+            pltpu.VMEM((chips, near_count, feats), BF16),
             pltpu.VMEM((groups, rows, feats), BF16),
+            pltpu.VMEM((peers, tokens, feats), BF16),
+            pltpu.VMEM((peers, tokens, feats), BF16),
             pltpu.VMEM(gate_weight.shape[1:], BF16),
             pltpu.VMEM(up_weight.shape[1:], BF16),
             dma((5,)),
@@ -686,20 +849,30 @@
             dma((sp_size,)),
             dma((sp_size,)),
             dma((sp_size,)),
-            dma((max(chips - 1, 1), pieces)),
+            dma((peers, pieces)),
             dma((chips, pieces)),
             dma((heads, tp_size)),
             dma((heads, tp_size)),
-            dma((sp_size,)),
-            dma((sp_size,)),
+            dma((peers,)),
+            dma((chips,)),
+            dma((reach, chips)),
+            dma((reach, chips)),
+            dma((reach,)),
+            dma((reach,)),
+            dma((chips,)),
+            dma((chips,)),
             dma((groups, tp_size)),
             dma((groups, tp_size)),
-            dma((groups,)),
-            dma((groups,)),
-            dma((groups, max(chips - 1, 1))),
-            dma((groups, max(chips - 1, 1))),
-            dma((sp_size,)),
-            dma((sp_size,)),
+            dma((groups + 1,)),
+            dma((groups + 1,)),
+            dma((groups, peers)),
+            dma((groups, peers)),
+            dma((reach, chips)),
+            dma((reach, chips)),
+            dma((reach,)),
+            dma((reach,)),
+            dma((peers,)),
+            dma((peers,)),
         ],
         compiler_params=pltpu.CompilerParams(
             collective_id=0, has_side_effects=True, vmem_limit_bytes=56 * 1024 * 1024

time: 117 us -> 119 us (1.017)
  Pallas kernels: 115 us -> 117 us
    pallas_call x1, Pallas kernels: 115 us -> 117 us  [local(): pl.pallas_call(functools.partial(layer_kernel, sp_size, tp_size, groups,...]
where the time goes in v3:
time: 119 us
  Pallas kernels  117 us (98%)
  local copies, waits for them, and re-layouts  1.62 us (1%)
    pallas_call x1, Pallas kernels, local(): pl.pallas_call(functools.partial(layer_kernel, sp_size, tp_size, groups,...  117 us

profile of v3, /device:TPU:0, one launch (start us, length us, event | category | flops | bytes accessed | tf_op | source)
XLA Modules:
  0.0 118.5 jit_solution(2816751923622488100)
XLA Ops:
  0.0 116.9 %shard_map.127 = bf16[192,512]{1,0:T(8,128)(2,1)} custom-call(bf16[192,512]{1,0:T(8,128)(2,1)} %residual_hbm.1, bf16[192,4,128]{2,1,0:T(4,128)(2,1)} %query_hbm.1, bf16[192,4,128]{2,1,0:T(4,128)(2,1)} %key_hbm.1, bf16[192,4,128]{2,1,0:T(4,128)(2,1)} %value_hbm.1, f32[4]{0:T(128)} %diff_scale.1, f32[1,128]{1,0:T(1,128)} %bitcast.13, ...), custom_call_target="tpu_custom_call" | custom-call | tf_op jit(solution)/shard_map/pallas_call | solution.py:797
  116.9 1.6 %copy.15 = bf16[192,512]{1,0:T(8,128)(2,1)} copy(bf16[192,512]{1,0:T(8,128)(2,1)} %shard_map.127) | data formatting | bytes 393216

commit v4 on v3

--- a/solution.py
+++ b/solution.py
@@ -78,6 +78,8 @@
     along_send,
     across_send,
     kv_recv,
+    rest_send,
+    rest_recv,
     down_send,
     down_recv,
     att_send,
@@ -113,6 +115,7 @@
     half_of = me // reach
     spot = lax.rem(me, reach)
     span = reach // groups
+    ahead = (groups + 1) // 2
     rows = span * cap
     near_count = reach * cap
     tokens, heads, width = query_hbm.shape
@@ -191,7 +194,7 @@
 
     for i in range(2):
         raw_loads[i].wait()
-        blocks[me, i] = jnp.transpose(raw[i], (1, 0, 2))
+        blocks[me, :, i] = jnp.transpose(raw[i], (1, 0, 2))
     raw_loads[2].wait()
     low = lax.broadcasted_iota(jnp.int32, (heads, tokens, width), 2) < QK
     query = jnp.transpose(raw[2], (1, 0, 2)).astype(F32) * QK ** (-0.5)
@@ -225,6 +228,17 @@
         return remote(
             blocks.at[block], blocks.at[block], send.at[back], kv_recv.at[block], at(target)
         )
+
+    top = pairs - 1
+    kept = heads // 2 if heads % 2 == 0 and pairs > 1 else heads
+
+    def kept_part(block, send, back, target):
+        part = blocks.at[block, pl.ds(0, kept)]
+        return remote(part, part, send.at[back], kv_recv.at[block], at(target))
+
+    def rest_part(target):
+        part = blocks.at[0, pl.ds(kept, heads - kept)]
+        return remote(part, part, rest_send, rest_recv, at(target))
 
     def attend(block, masked):
         if masked:
@@ -233,11 +247,11 @@
             visible = key // SPAN <= query // SPAN
         for head in range(heads):
             value = jnp.concatenate(
-                [jnp.transpose(blocks[block, 1, head]), jnp.ones((16, tokens), BF16)], axis=0
+                [jnp.transpose(blocks[block, head, 1]), jnp.ones((16, tokens), BF16)], axis=0
             )
             for half in range(2):
                 scores = lax.dot_general(
-                    blocks[block, 0, head],
+                    blocks[block, head, 0],
                     scaled[half, head],
                     (((1,), (1,)), ((), ())),
                     preferred_element_type=F32,
@@ -271,9 +285,15 @@
             def _():
                 hand_on(block, along_send, back, me + 2).start()
 
-            @pl.when((back > 0) | (side == 0))
+            cut = (pair == top) & (side == 0) & (back == pair) & (kept < heads)
+
+            @pl.when(((back > 0) | (side == 0)) & jnp.logical_not(cut))
             def _():
                 hand_on(block, across_send, back, other).start()
+
+            @pl.when(cut)
+            def _():
+                kept_part(block, across_send, back, other).start()
 
         @pl.when(back == 0)
         def _():
@@ -287,9 +307,21 @@
 
         @pl.loop(0, 2)
         def _(which):
-            @pl.when((which == 1) & use_second)
+            parted = (me == sp_size - 1) & (second == 0) & (kept < heads)
+
+            @pl.when((which == 1) & use_second & jnp.logical_not(parted))
             def _():
                 hand_on(second, across_send, 0, other).wait_recv()
+
+            if kept < heads:
+                @pl.when((which == 1) & use_second & parted)
+                def _():
+                    kept_part(second, across_send, 0, other).wait_recv()
+                    rest_part(other).wait_recv()
+
+                @pl.when((which == 1) & use_second & (me == sp_size - 3) & (second == 0))
+                def _():
+                    rest_part(me + 2).start()
 
             @pl.when(((which == 0) & (back > 0) & (back <= pair)) | ((which == 1) & use_second))
             def _():
@@ -317,8 +349,6 @@
         onward.start()
 
     def collect(buffer, send, recv):
-        for step in range(1, chips):
-            forward(buffer, send, recv, step)
         for step in range(chips):
             owner = peer_rank(step) + 1 - 2 * parity
             piece(buffer, send, recv, owner, sibling, sibling).wait_recv()
@@ -331,17 +361,18 @@
         piece(buffer, send, recv, rank, sibling, sibling).wait_send()
 
     for head in range(heads):
-        maps = [
-            accum[index, :width] / accum[index, width : width + 1]
-            for index in (head * 2, head * 2 + 1)
+        shrink = [
+            1.0 / accum[index, width : width + 1] for index in (head * 2, head * 2 + 1)
         ]
-        mixture = maps[0] - diff_scale[head] * maps[1]
+        mixture = (
+            accum[head * 2, :width] * shrink[0]
+            - accum[head * 2 + 1, :width] * (diff_scale[head] * shrink[1])
+        )
         scale_back = lax.rsqrt(jnp.mean(mixture * mixture, axis=0, keepdims=True) + NORM_EPS)
         heads_all[head, rank] = (
             jnp.transpose(mixture * scale_back) * head_gain[...] * HEAD_KEEP
         ).astype(BF16)
         spread(heads_all.at[head], att_send.at[head], att_recv.at[head])
-    send_down(early, pieces)
     weights[0].wait()
     weights[4].wait()
 
@@ -352,7 +383,7 @@
             preferred_element_type=F32,
         )
 
-    sums = own_sum
+    sums = updated
     sums[...] = residual[...].astype(F32) + project(rank)
     for head in range(heads):
         for step in range(1, chips):
@@ -366,6 +397,7 @@
             ).wait_recv()
         return project(owner)
 
+    send_down(early, early + 1)
     sums[...] += from_sibling(0)
     for step in range(1, chips):
         sums[...] += project(peer_rank(step))
@@ -428,12 +460,15 @@
             near_out[place, source] = chosen_rows(place, source)
             near_dispatch(place, source).start()
 
-    @pl.loop(0, reach)
-    def _(place):
-        far_out[place] = chosen_rows(reach + place, chip)
-        far_dispatch(place).start()
-
+    def send_far(first, last):
+        @pl.loop(first, last)
+        def _(place):
+            far_out[place] = chosen_rows(reach + place, chip)
+            far_dispatch(place).start()
+
+    send_far(0, span)
     send_near(chip)
+    send_far(span, span * ahead)
     for step in range(1, chips):
         source = lax.rem(chip + step, chips)
         remote(
@@ -443,7 +478,10 @@
             mix_recv.at[source],
             beside(sibling),
         ).wait_recv()
+        if step == 1:
+            send_down(early + 1, early + 2)
         send_near(source)
+    send_far(span * ahead, reach)
 
     unit_tile = math.gcd(units, 256)
     column_tile = math.gcd(columns, 256)
@@ -504,7 +542,7 @@
             beside(sibling),
         )
 
-    def run_up(table, hidden, count, index):
+    def run_up(table, hidden, count, index, beat=None):
         square = 0.0
         for part in range(tp_size):
             value = table[part].astype(F32)
@@ -525,16 +563,22 @@
             linear = jnp.clip(pre_up, -CLAMP_LIMIT, CLAMP_LIMIT)
             value = capped * jax.nn.sigmoid(SWISH_ALPHA * capped) * (linear + 1.0)
             hidden[parity, :, cols] = value.astype(BF16)
+            if beat is not None:
+                beat(tile)
 
         hidden_copy(hidden, index, parity).start()
 
-    def far_up(group):
+    def hand_over(group):
+        for step in range(1, chips):
+            forward(far_rows.at[group], row_send.at[group], row_recv.at[group], step)
+
+    def far_up(group, beat=None):
         collect(far_rows.at[group], row_send.at[group], row_recv.at[group])
-        run_up(far_rows.at[group], far_hidden.at[group], rows, group)
-
-    def near_up():
+        run_up(far_rows.at[group], far_hidden.at[group], rows, group, beat)
+
+    def near_up(beat):
         pair_wait()
-        run_up(near_rows, near_hidden, near_count, groups)
+        run_up(near_rows, near_hidden, near_count, groups, beat)
 
     def sum_copy(group, step):
         target = lax.rem(chip + step, chips)
@@ -635,37 +679,47 @@
         for place in range(span):
             give_back(group * span + place).start()
 
-    spread_rows(0)
-    pair_rows()
+    def at_tiles(acts):
+        def beat(tile):
+            for number, act in acts:
+                pl.when(tile == number)(act)
+
+        return beat
+
+    last_tile = units // unit_tile - 1
+    first_part = list(range(ahead))
+    second_part = list(range(ahead, groups))
+
+    def second_out():
+        for group in second_part:
+            spread_rows(group)
+
+    def first_done():
+        for group in first_part:
+            finish(group)
+
     weights[1].wait()
     weights[2].wait()
-    near_up()
-
-    @pl.loop(0, groups + 2)
-    def _(turn):
-        @pl.when(turn < groups - 1)
-        def _():
-            spread_rows(turn + 1)
-
-        @pl.when(turn < groups)
-        def _():
-            far_up(turn)
-
-        @pl.when(turn == 1)
-        def _():
-            down_ready()
-
-        @pl.when(turn >= 2)
-        def _():
-            finish(turn - 2)
-
-        @pl.when((turn >= 1) & (turn < groups + 1))
-        def _():
-            far_down(turn - 1)
-
-        @pl.when(turn == 1)
-        def _():
-            near_down()
+    for group in first_part:
+        spread_rows(group)
+    pair_rows()
+    send_down(early + 2, pieces)
+    for group in first_part:
+        hand_over(group)
+    for group in first_part:
+        far_up(group)
+    near_up(at_tiles([(0, second_out)]))
+    down_ready()
+    for group in first_part:
+        far_down(group)
+    for group in second_part:
+        hand_over(group)
+        far_up(group, at_tiles([(last_tile, first_done)]))
+    for group in second_part:
+        far_down(group)
+    near_down()
+    for group in second_part:
+        finish(group)
 
     def routed_sum(first, count, table):
         portion = 0.0
@@ -712,7 +766,6 @@
     for step in range(1, chips):
         share_copy(step).wait_recv()
         sums[...] += share_recv[step - 1].astype(F32)
-    updated[...] = sums[...].astype(BF16)
 
     @pl.loop(0, pair + 1)
     def _(back):
@@ -722,9 +775,20 @@
         def _():
             hand_on(block, along_send, back, me + 2).wait_send()
 
-        @pl.when((back > 0) | (side == 0))
+        cut = (pair == top) & (side == 0) & (back == pair) & (kept < heads)
+
+        @pl.when(((back > 0) | (side == 0)) & jnp.logical_not(cut))
         def _():
             hand_on(block, across_send, back, other).wait_send()
+
+        @pl.when(cut)
+        def _():
+            kept_part(block, across_send, back, other).wait_send()
+
+    if kept < heads:
+        @pl.when(me == sp_size - 3)
+        def _():
+            rest_part(me + 2).wait_send()
 
     for step in range(1, chips):
         @pl.loop(0, pieces)
@@ -783,20 +847,20 @@
     tops = expert_ids.shape[1]
     cap = -(-(2 * tokens * tops // sp_size) // 16) * 16
     reach = sp_size // 2
-    groups = math.gcd(reach, 4)
+    groups = math.gcd(reach, 2)
     rows = reach // groups * cap
     near_count = reach * cap
     units = gate_weight.shape[2]
     chips = tp_size // 2
     peers = max(chips - 1, 1)
     pieces = 16
-    early = 13
+    early = 12
     dma = pltpu.SemaphoreType.DMA
     vmem = pl.BlockSpec(memory_space=pltpu.VMEM)
     hbm = pl.BlockSpec(memory_space=pl.ANY)
     return pl.pallas_call(
         functools.partial(layer_kernel, sp_size, tp_size, groups, cap, early),
-        out_shape=jax.ShapeDtypeStruct((tokens, feats), BF16),
+        out_shape=jax.ShapeDtypeStruct((tokens, feats), F32),
         in_specs=[
             hbm,
             hbm,
@@ -817,7 +881,7 @@
             pltpu.VMEM((tokens, feats), BF16),
             pltpu.VMEM((3, tokens, heads, width), BF16),
             pltpu.VMEM((2, heads, tokens, width), BF16),
-            pltpu.VMEM((sp_size, 2, heads, tokens, width), BF16),
+            pltpu.VMEM((sp_size, heads, 2, tokens, width), BF16),
             pltpu.VMEM((heads * 2, 1, tokens), F32),
             pltpu.VMEM((heads * 2, width + 16, tokens), F32),
             pltpu.VMEM((heads, tp_size, tokens, width), BF16),
@@ -849,6 +913,8 @@
             dma((sp_size,)),
             dma((sp_size,)),
             dma((sp_size,)),
+            dma(()),
+            dma(()),
             dma((peers, pieces)),
             dma((chips, pieces)),
             dma((heads, tp_size)),
@@ -891,7 +957,7 @@
         down_weight[0],
         expert_ids.T,
         route_logit.T,
-    )
+    ).astype(BF16)
 
 
 def solution(mesh):

time: 119 us -> 108 us (0.908)
  Pallas kernels: 117 us -> 105 us
  other arithmetic: 0 us -> 1.7 us
  local copies, waits for them, and re-layouts: 1.62 us -> 0 us
    pallas_call x1, Pallas kernels: 117 us -> 105 us  [local(): pl.pallas_call(functools.partial(layer_kernel, sp_size, tp_size, groups,...]
    convert_element_type x0 -> x1, other arithmetic: none -> 1.7 us  [local(): return pl.pallas_call(functools.partial(layer_kernel, sp_size, tp_size, g...]
    unnamed x1 -> x0, local copies, waits for them, and re-layouts: 1.62 us -> none
where the time goes in v4:
time: 108 us; the launch traced here: 107 us
  Pallas kernels  105 us (97%)
  other arithmetic  1.7 us (2%)
    pallas_call x1, Pallas kernels, local(): pl.pallas_call(functools.partial(layer_kernel, sp_size, tp_size, groups,...  105 us

profile of v4, /device:TPU:0, one launch (start us, length us, event | category | flops | bytes accessed | tf_op | source)
XLA Modules:
  0.0 106.8 jit_solution(17557459794558530456)
XLA Ops:
  0.0 105.1 %shard_map.127 = f32[192,512]{1,0:T(8,128)} custom-call(bf16[192,512]{1,0:T(8,128)(2,1)} %residual_hbm.1, bf16[192,4,128]{2,1,0:T(4,128)(2,1)} %query_hbm.1, bf16[192,4,128]{2,1,0:T(4,128)(2,1)} %key_hbm.1, bf16[192,4,128]{2,1,0:T(4,128)(2,1)} %value_hbm.1, f32[4]{0:T(128)} %diff_scale.1, f32[1,128]{1,0:T(1,128)} %bitcast.13, bf16[2048,512]{1,0:T(8,128)(2,1)} %out_hbm.1, ...), custom_call_target="tpu_custom_call" | custom-call | tf_op jit(solution)/shard_map/pallas_call | solution.py:861
  105.1 1.7 %convert_element_type.3 = bf16[192,512]{1,0:T(8,128)(2,1)} convert(f32[192,512]{1,0:T(8,128)} %shard_map.127) | non-fusion elementwise | flops 98304 | bytes 589824 | tf_op jit(solution)/shard_map/convert_element_type | solution.py:960

commit v5 on v4

--- a/solution.py
+++ b/solution.py
@@ -28,7 +28,8 @@
     tp_size,
     groups,
     cap,
-    early,
+    ext,
+    chunk,
     residual_hbm,
     query_hbm,
     key_hbm,
@@ -60,7 +61,10 @@
     normed,
     near_hidden,
     far_hidden,
+    far_ext,
+    near_ext,
     down_part,
+    down_ext,
     own_sum,
     far_sum,
     part_send,
@@ -96,6 +100,9 @@
     row_recv,
     hid_send,
     hid_recv,
+    ext_send,
+    ext_recv,
+    ext_over_send,
     sum_send,
     sum_recv,
     near_ret_send,
@@ -150,7 +157,8 @@
     for copy in raw_loads:
         copy.start()
     pieces = down_send.shape[1]
-    chunk = 2 * units // pieces
+    moved = units - ext
+    per_core = moved // chunk
     weights = [
         pltpu.make_async_copy(out_hbm, out_w, weight_sem.at[0]),
         pltpu.make_async_copy(gate_hbm, gate, weight_sem.at[1]),
@@ -160,6 +168,17 @@
         ),
         pltpu.make_async_copy(residual_hbm, residual, weight_sem.at[4]),
     ]
+    if ext:
+        for step in range(1, chips):
+            for core in range(2):
+                start = (lax.rem(chip + step, chips) * 2 + core) * units + moved
+                weights.append(
+                    pltpu.make_async_copy(
+                        down_hbm.at[pl.ds(start, ext)],
+                        down_ext.at[step - 1, pl.ds(core * ext, ext)],
+                        weight_sem.at[5 + (step - 1) * 2 + core],
+                    )
+                )
 
     barrier = pltpu.get_barrier_semaphore()
     for step in range(1, sp_size):
@@ -203,11 +222,14 @@
 
     pl.semaphore_wait(barrier, sp_size - 1 + chips)
 
+    def piece_row(piece):
+        return piece // per_core * units + lax.rem(piece, per_core) * chunk
+
     def down_piece(step, piece):
         target = lax.rem(chip + step, chips)
         return remote(
-            down_hbm.at[pl.ds(target * 2 * units + piece * chunk, chunk)],
-            down_part.at[chip, pl.ds(piece * chunk, chunk)],
+            down_hbm.at[pl.ds(target * 2 * units + piece_row(piece), chunk)],
+            down_part.at[chip, pl.ds(piece_row(piece), chunk)],
             down_send.at[step - 1, piece],
             down_recv.at[chip, piece],
             beside(target * 2 + parity),
@@ -230,14 +252,14 @@
         )
 
     top = pairs - 1
-    kept = heads // 2 if heads % 2 == 0 and pairs > 1 else heads
+    kept = heads // 2 if heads % 2 == 0 and pairs > 2 else heads
 
     def kept_part(block, send, back, target):
         part = blocks.at[block, pl.ds(0, kept)]
         return remote(part, part, send.at[back], kv_recv.at[block], at(target))
 
-    def rest_part(target):
-        part = blocks.at[0, pl.ds(kept, heads - kept)]
+    def rest_part(block, target):
+        part = blocks.at[block, pl.ds(kept, heads - kept)]
         return remote(part, part, rest_send, rest_recv, at(target))
 
     def attend(block, masked):
@@ -285,7 +307,7 @@
             def _():
                 hand_on(block, along_send, back, me + 2).start()
 
-            cut = (pair == top) & (side == 0) & (back == pair) & (kept < heads)
+            cut = (pair == top) & (back == pair) & (kept < heads)
 
             @pl.when(((back > 0) | (side == 0)) & jnp.logical_not(cut))
             def _():
@@ -297,7 +319,7 @@
 
         @pl.when(back == 0)
         def _():
-            send_down(0, early)
+            send_down(0, pieces - 2)
             for copy in weights:
                 copy.start()
             attend(me, True)
@@ -307,7 +329,8 @@
 
         @pl.loop(0, 2)
         def _(which):
-            parted = (me == sp_size - 1) & (second == 0) & (kept < heads)
+            final = second == other - 2 * pair
+            parted = (pair == top) & final & (kept < heads)
 
             @pl.when((which == 1) & use_second & jnp.logical_not(parted))
             def _():
@@ -317,11 +340,11 @@
                 @pl.when((which == 1) & use_second & parted)
                 def _():
                     kept_part(second, across_send, 0, other).wait_recv()
-                    rest_part(other).wait_recv()
-
-                @pl.when((which == 1) & use_second & (me == sp_size - 3) & (second == 0))
+                    rest_part(second, other).wait_recv()
+
+                @pl.when((which == 1) & use_second & (pair == top - 1) & final)
                 def _():
-                    rest_part(me + 2).start()
+                    rest_part(second, me + 2).start()
 
             @pl.when(((which == 0) & (back > 0) & (back <= pair)) | ((which == 1) & use_second))
             def _():
@@ -397,7 +420,7 @@
             ).wait_recv()
         return project(owner)
 
-    send_down(early, early + 1)
+    send_down(pieces - 2, pieces - 1)
     sums[...] += from_sibling(0)
     for step in range(1, chips):
         sums[...] += project(peer_rank(step))
@@ -478,8 +501,6 @@
             mix_recv.at[source],
             beside(sibling),
         ).wait_recv()
-        if step == 1:
-            send_down(early + 1, early + 2)
         send_near(source)
     send_far(span * ahead, reach)
 
@@ -542,7 +563,44 @@
             beside(sibling),
         )
 
-    def run_up(table, hidden, count, index, beat=None):
+    def ext_copy(hidden, extra, index, step):
+        target = lax.rem(chip + step, chips)
+        return remote(
+            hidden.at[parity, :, pl.ds(moved, ext)],
+            extra.at[chip, parity],
+            ext_send.at[index, step - 1],
+            ext_recv.at[index, chip, parity],
+            beside(target * 2 + parity),
+        )
+
+    def ext_onward(extra, index, step, core):
+        source = lax.rem(chip + step, chips)
+        return remote(
+            extra.at[source, core],
+            extra.at[source, core],
+            ext_over_send.at[index, step - 1],
+            ext_recv.at[index, source, core],
+            beside(sibling),
+        )
+
+    def ext_over(extra, index):
+        if ext:
+            for step in range(1, chips):
+                onward = ext_onward(extra, index, step, parity)
+                onward.wait_recv()
+                onward.start()
+
+    def ext_wait(extra, index):
+        if ext:
+            for step in range(1, chips):
+                ext_onward(extra, index, step, 1 - parity).wait_recv()
+
+    def send_ext(hidden, extra, index):
+        if ext:
+            for step in range(1, chips):
+                ext_copy(hidden, extra, index, step).start()
+
+    def run_up(table, hidden, extra, count, index, beat=None):
         square = 0.0
         for part in range(tp_size):
             value = table[part].astype(F32)
@@ -556,13 +614,19 @@
 
         @pl.loop(0, units // unit_tile)
         def _(tile):
-            cols = pl.ds(pl.multiple_of(tile * unit_tile, unit_tile), unit_tile)
+            turned = lax.rem(tile + moved // unit_tile, units // unit_tile)
+            cols = pl.ds(pl.multiple_of(turned * unit_tile, unit_tile), unit_tile)
             pre_gate = jnp.dot(normed[:count], gate[:, cols], preferred_element_type=F32)
             pre_up = jnp.dot(normed[:count], up[:, cols], preferred_element_type=F32)
             capped = jnp.minimum(pre_gate, CLAMP_LIMIT)
             linear = jnp.clip(pre_up, -CLAMP_LIMIT, CLAMP_LIMIT)
             value = capped * jax.nn.sigmoid(SWISH_ALPHA * capped) * (linear + 1.0)
             hidden[parity, :, cols] = value.astype(BF16)
+            if index is not groups:
+                @pl.when(tile == max(ext // unit_tile, 1) - 1)
+                def _():
+                    send_ext(hidden, extra, index)
+
             if beat is not None:
                 beat(tile)
 
@@ -574,11 +638,11 @@
 
     def far_up(group, beat=None):
         collect(far_rows.at[group], row_send.at[group], row_recv.at[group])
-        run_up(far_rows.at[group], far_hidden.at[group], rows, group, beat)
+        run_up(far_rows.at[group], far_hidden.at[group], far_ext.at[group], rows, group, beat)
 
     def near_up(beat):
         pair_wait()
-        run_up(near_rows, near_hidden, near_count, groups, beat)
+        run_up(near_rows, near_hidden, near_ext, near_count, groups, beat)
 
     def sum_copy(group, step):
         target = lax.rem(chip + step, chips)
@@ -594,10 +658,28 @@
         value = 0.0
         for core in range(2):
             value += jnp.dot(
-                hidden[core],
-                down_part[block, core * units : (core + 1) * units, cols],
+                hidden[core, :, :moved],
+                down_part[block, core * units : core * units + moved, cols],
                 preferred_element_type=F32,
             )
+        return value
+
+    def own_part(hidden, extra, cols):
+        value = 0.0
+        for core in range(2):
+            value += jnp.dot(
+                hidden[core],
+                down_part[chip, core * units : (core + 1) * units, cols],
+                preferred_element_type=F32,
+            )
+        if ext:
+            for step in range(1, chips):
+                for core in range(2):
+                    value += jnp.dot(
+                        extra[lax.rem(chip + step, chips), core],
+                        down_ext[step - 1, core * ext : (core + 1) * ext, cols],
+                        preferred_element_type=F32,
+                    )
         return value
 
     def column_loop(body):
@@ -613,14 +695,14 @@
             @pl.loop(0, pieces)
             def _(index):
                 remote(
-                    down_part.at[source, pl.ds(index * chunk, chunk)],
-                    down_part.at[source, pl.ds(index * chunk, chunk)],
+                    down_part.at[source, pl.ds(piece_row(index), chunk)],
+                    down_part.at[source, pl.ds(piece_row(index), chunk)],
                     down_send.at[step - 1, index],
                     down_recv.at[source, index],
                     beside(sibling),
                 ).wait_recv()
 
-    def far_down(group):
+    def far_outward(group):
         hidden_copy(far_hidden.at[group], group, 1 - parity).wait_recv()
         for step in range(1, chips):
             def outward(cols):
@@ -631,8 +713,11 @@
             column_loop(outward)
             sum_copy(group, step).start()
 
+    def far_inward(group):
+        ext_wait(far_ext.at[group], group)
+
         def inward(cols):
-            far_sum[group, :, cols] = part_sum(far_hidden.at[group], chip, cols)
+            far_sum[group, :, cols] = own_part(far_hidden.at[group], far_ext.at[group], cols)
 
         column_loop(inward)
 
@@ -645,13 +730,19 @@
             near_at(place),
         )
 
-    def near_down():
-        hidden_copy(near_hidden, groups, 1 - parity).wait_recv()
-        for step in range(1, chips + 1):
+    def near_down(steps):
+        for step in steps:
             block = lax.rem(chip + step, chips)
 
+            if step == chips:
+                ext_wait(near_ext, groups)
+
             def store(cols):
-                near_result[block, :, cols] = part_sum(near_hidden, block, cols).astype(BF16)
+                if step < chips:
+                    value = part_sum(near_hidden, block, cols)
+                else:
+                    value = own_part(near_hidden, near_ext, cols)
+                near_result[block, :, cols] = value.astype(BF16)
 
             column_loop(store)
 
@@ -694,6 +785,13 @@
         for group in second_part:
             spread_rows(group)
 
+    def first_ext():
+        for group in first_part:
+            ext_over(far_ext.at[group], group)
+
+    def near_ext_out():
+        send_ext(near_hidden, near_ext, groups)
+
     def first_done():
         for group in first_part:
             finish(group)
@@ -702,24 +800,97 @@
     weights[2].wait()
     for group in first_part:
         spread_rows(group)
-    pair_rows()
-    send_down(early + 2, pieces)
-    for group in first_part:
         hand_over(group)
+    send_down(pieces - 1, pieces)
     for group in first_part:
         far_up(group)
-    near_up(at_tiles([(0, second_out)]))
+    pair_rows()
     down_ready()
     for group in first_part:
-        far_down(group)
+        far_outward(group)
+    near_up(at_tiles([(0, second_out), (1, first_ext), (last_tile, near_ext_out)]))
+    for copy in weights[5:]:
+        copy.wait()
+    for group in first_part:
+        far_inward(group)
+    first_done()
+    hidden_copy(near_hidden, groups, 1 - parity).wait_recv()
+    near_down(range(1, chips))
     for group in second_part:
         hand_over(group)
-        far_up(group, at_tiles([(last_tile, first_done)]))
     for group in second_part:
-        far_down(group)
-    near_down()
+        far_up(group)
+    ext_over(near_ext, groups)
+    for group in second_part:
+        far_outward(group)
+    near_down((chips,))
+    for group in second_part:
+        ext_over(far_ext.at[group], group)
+    for group in second_part:
+        far_inward(group)
     for group in second_part:
         finish(group)
+
+    @pl.loop(0, pair + 1)
+    def _(back):
+        block = me - 2 * back
+
+        @pl.when(pair < pairs - 1)
+        def _():
+            hand_on(block, along_send, back, me + 2).wait_send()
+
+        cut = (pair == top) & (back == pair) & (kept < heads)
+
+        @pl.when(((back > 0) | (side == 0)) & jnp.logical_not(cut))
+        def _():
+            hand_on(block, across_send, back, other).wait_send()
+
+        @pl.when(cut)
+        def _():
+            kept_part(block, across_send, back, other).wait_send()
+
+    if kept < heads:
+        @pl.when(pair == top - 1)
+        def _():
+            rest_part(other - 2 * pair, me + 2).wait_send()
+
+    for step in range(1, chips):
+        @pl.loop(0, pieces)
+        def _(index):
+            down_piece(step, index).wait_send()
+
+    for head in range(heads):
+        settle(heads_all.at[head], att_send.at[head], att_recv.at[head])
+
+    for step in range(1, chips):
+        mix_copy(step).wait_send()
+
+    @pl.loop(0, reach)
+    def _(place):
+        far_dispatch(place).wait_send()
+
+    for source in range(chips):
+        pair_copy(source).wait_send()
+
+        @pl.loop(1, reach)
+        def _(place):
+            near_dispatch(place, source).wait_send()
+
+    hidden_copy(near_hidden, groups, parity).wait_send()
+    if ext:
+        for step in range(1, chips):
+            ext_copy(near_hidden, near_ext, groups, step).wait_send()
+            ext_onward(near_ext, groups, step, parity).wait_send()
+
+    @pl.loop(0, groups)
+    def _(group):
+        settle(far_rows.at[group], row_send.at[group], row_recv.at[group])
+        hidden_copy(far_hidden.at[group], group, parity).wait_send()
+        for step in range(1, chips):
+            if ext:
+                ext_copy(far_hidden.at[group], far_ext.at[group], group, step).wait_send()
+                ext_onward(far_ext.at[group], group, step, parity).wait_send()
+            sum_copy(group, step).wait_send()
 
     def routed_sum(first, count, table):
         portion = 0.0
@@ -767,62 +938,17 @@
         share_copy(step).wait_recv()
         sums[...] += share_recv[step - 1].astype(F32)
 
-    @pl.loop(0, pair + 1)
-    def _(back):
-        block = me - 2 * back
-
-        @pl.when(pair < pairs - 1)
-        def _():
-            hand_on(block, along_send, back, me + 2).wait_send()
-
-        cut = (pair == top) & (side == 0) & (back == pair) & (kept < heads)
-
-        @pl.when(((back > 0) | (side == 0)) & jnp.logical_not(cut))
-        def _():
-            hand_on(block, across_send, back, other).wait_send()
-
-        @pl.when(cut)
-        def _():
-            kept_part(block, across_send, back, other).wait_send()
-
-    if kept < heads:
-        @pl.when(me == sp_size - 3)
-        def _():
-            rest_part(me + 2).wait_send()
-
     for step in range(1, chips):
-        @pl.loop(0, pieces)
-        def _(index):
-            down_piece(step, index).wait_send()
-
-    for head in range(heads):
-        settle(heads_all.at[head], att_send.at[head], att_recv.at[head])
-
-    for step in range(1, chips):
-        mix_copy(step).wait_send()
         share_copy(step).wait_send()
 
     @pl.loop(0, reach)
     def _(place):
-        far_dispatch(place).wait_send()
         give_back(place).wait_send()
 
     for source in range(chips):
-        pair_copy(source).wait_send()
-
         @pl.loop(1, reach)
         def _(place):
-            near_dispatch(place, source).wait_send()
             near_return(place, source).wait_send()
-
-    hidden_copy(near_hidden, groups, parity).wait_send()
-
-    @pl.loop(0, groups)
-    def _(group):
-        settle(far_rows.at[group], row_send.at[group], row_recv.at[group])
-        hidden_copy(far_hidden.at[group], group, parity).wait_send()
-        for step in range(1, chips):
-            sum_copy(group, step).wait_send()
 
 
 def local(
@@ -853,13 +979,15 @@
     units = gate_weight.shape[2]
     chips = tp_size // 2
     peers = max(chips - 1, 1)
-    pieces = 16
-    early = 12
+    chunk = 2 * units // 16
+    ext = units // 8 if units % 1024 == 0 else 0
+    kept_ext = max(ext, 128)
+    pieces = 2 * ((units - ext) // chunk)
     dma = pltpu.SemaphoreType.DMA
     vmem = pl.BlockSpec(memory_space=pltpu.VMEM)
     hbm = pl.BlockSpec(memory_space=pl.ANY)
     return pl.pallas_call(
-        functools.partial(layer_kernel, sp_size, tp_size, groups, cap, early),
+        functools.partial(layer_kernel, sp_size, tp_size, groups, cap, ext, chunk),
         out_shape=jax.ShapeDtypeStruct((tokens, feats), F32),
         in_specs=[
             hbm,
@@ -895,7 +1023,10 @@
             pltpu.VMEM((near_count, tp_size * feats), BF16),
             pltpu.VMEM((2, near_count, units), BF16),
             pltpu.VMEM((groups, 2, rows, units), BF16),
+            pltpu.VMEM((groups, chips, 2, rows, kept_ext), BF16),
+            pltpu.VMEM((chips, 2, near_count, kept_ext), BF16),
             pltpu.VMEM((chips, 2 * units, feats), BF16),
+            pltpu.VMEM((peers, 2 * kept_ext, feats), BF16),
             pltpu.VMEM((tokens, feats), F32),
             pltpu.VMEM((groups, rows, feats), F32),
             pltpu.VMEM((groups, peers, rows, feats), BF16),
@@ -908,7 +1039,7 @@
             pltpu.VMEM((peers, tokens, feats), BF16),
             pltpu.VMEM(gate_weight.shape[1:], BF16),
             pltpu.VMEM(up_weight.shape[1:], BF16),
-            dma((5,)),
+            dma((5 + 2 * peers,)),
             dma((3,)),
             dma((sp_size,)),
             dma((sp_size,)),
@@ -931,6 +1062,9 @@
             dma((groups, tp_size)),
             dma((groups + 1,)),
             dma((groups + 1,)),
+            dma((groups + 1, peers)),
+            dma((groups + 1, chips, 2)),
+            dma((groups + 1, peers)),
             dma((groups, peers)),
             dma((groups, peers)),
             dma((reach, chips)),

time: 108 us -> 107 us (level)
  no operation moved by 1% of the time
where the time goes in v5:
time: 107 us
  Pallas kernels  105 us (98%)
  other arithmetic  1.7 us (2%)
    pallas_call x1, Pallas kernels, local(): pl.pallas_call(functools.partial(layer_kernel, sp_size, tp_size, groups,...  105 us

profile of v5, /device:TPU:0, one launch (start us, length us, event | category | flops | bytes accessed | tf_op | source)
XLA Modules:
  0.0 106.7 jit_solution(17307785558683993843)
XLA Ops:
  0.0 105.0 %shard_map.127 = f32[192,512]{1,0:T(8,128)} custom-call(bf16[192,512]{1,0:T(8,128)(2,1)} %residual_hbm.1, bf16[192,4,128]{2,1,0:T(4,128)(2,1)} %query_hbm.1, bf16[192,4,128]{2,1,0:T(4,128)(2,1)} %key_hbm.1, bf16[192,4,128]{2,1,0:T(4,128)(2,1)} %value_hbm.1, f32[4]{0:T(128)} %diff_scale.1, f32[1,128]{1,0:T(1,128)} %bitcast.13, bf16[2048,512]{1,0:T(8,128)(2,1)} %out_hbm.1, ...), custom_call_target="tpu_custom_call" | custom-call | tf_op jit(solution)/shard_map/pallas_call | solution.py:989
  105.0 1.7 %convert_element_type.3 = bf16[192,512]{1,0:T(8,128)(2,1)} convert(f32[192,512]{1,0:T(8,128)} %shard_map.127) | non-fusion elementwise | flops 98304 | bytes 589824 | tf_op jit(solution)/shard_map/convert_element_type | solution.py:1094

commit v6 on v5

--- a/solution.py
+++ b/solution.py
@@ -507,8 +507,16 @@
     unit_tile = math.gcd(units, 256)
     column_tile = math.gcd(columns, 256)
 
+    def row_part(group, place):
+        return (
+            far_rows.at[group, :, pl.ds(place * cap, cap)],
+            row_send.at[group, place],
+            row_recv.at[group, place],
+        )
+
     def spread_rows(group):
-        for place in range(span):
+        @pl.loop(0, span)
+        def _(place):
             remote(
                 far_out.at[0],
                 far_rows.at[group, rank, pl.ds(place * cap, cap)],
@@ -516,7 +524,7 @@
                 far_recv.at[group * span + place],
                 beside(sibling),
             ).wait_recv()
-        spread(far_rows.at[group], row_send.at[group], row_recv.at[group])
+            spread(*row_part(group, place))
 
     def pair_copy(source):
         return remote(
@@ -633,11 +641,16 @@
         hidden_copy(hidden, index, parity).start()
 
     def hand_over(group):
-        for step in range(1, chips):
-            forward(far_rows.at[group], row_send.at[group], row_recv.at[group], step)
+        @pl.loop(0, span)
+        def _(place):
+            for step in range(1, chips):
+                forward(*row_part(group, place), step)
 
     def far_up(group, beat=None):
-        collect(far_rows.at[group], row_send.at[group], row_recv.at[group])
+        @pl.loop(0, span)
+        def _(place):
+            collect(*row_part(group, place))
+
         run_up(far_rows.at[group], far_hidden.at[group], far_ext.at[group], rows, group, beat)
 
     def near_up(beat):
@@ -884,7 +897,10 @@
 
     @pl.loop(0, groups)
     def _(group):
-        settle(far_rows.at[group], row_send.at[group], row_recv.at[group])
+        @pl.loop(0, span)
+        def _(place):
+            settle(*row_part(group, place))
+
         hidden_copy(far_hidden.at[group], group, parity).wait_send()
         for step in range(1, chips):
             if ext:
@@ -980,7 +996,7 @@
     chips = tp_size // 2
     peers = max(chips - 1, 1)
     chunk = 2 * units // 16
-    ext = units // 8 if units % 1024 == 0 else 0
+    ext = units // 4 if units % 1024 == 0 else 0
     kept_ext = max(ext, 128)
     pieces = 2 * ((units - ext) // chunk)
     dma = pltpu.SemaphoreType.DMA
@@ -1058,8 +1074,8 @@
             dma((reach,)),
             dma((chips,)),
             dma((chips,)),
-            dma((groups, tp_size)),
-            dma((groups, tp_size)),
+            dma((groups, reach // groups, tp_size)),
+            dma((groups, reach // groups, tp_size)),
             dma((groups + 1,)),
             dma((groups + 1,)),
             dma((groups + 1, peers)),

time: 107 us -> 101 us (0.944)
  Pallas kernels: 105 us -> 98.4 us
    pallas_call x1, Pallas kernels: 105 us -> 98.4 us  [local(): pl.pallas_call(functools.partial(layer_kernel, sp_size, tp_size, groups,...]
where the time goes in v6:
time: 101 us; the launch traced here: 100 us
  Pallas kernels  98.4 us (97%)
  other arithmetic  1.7 us (2%)
    pallas_call x1, Pallas kernels, local(): pl.pallas_call(functools.partial(layer_kernel, sp_size, tp_size, groups,...  98.4 us

profile of v6, /device:TPU:0, one launch (start us, length us, event | category | flops | bytes accessed | tf_op | source)
XLA Modules:
  0.0 100.1 jit_solution(8525918445193382049)
XLA Ops:
  0.0 98.4 %shard_map.127 = f32[192,512]{1,0:T(8,128)} custom-call(bf16[192,512]{1,0:T(8,128)(2,1)} %residual_hbm.1, bf16[192,4,128]{2,1,0:T(4,128)(2,1)} %query_hbm.1, bf16[192,4,128]{2,1,0:T(4,128)(2,1)} %key_hbm.1, bf16[192,4,128]{2,1,0:T(4,128)(2,1)} %value_hbm.1, f32[4]{0:T(128)} %diff_scale.1, f32[1,128]{1,0:T(1,128)} %bitcast.13, bf16[2048,512]{1,0:T(8,128)(2,1)} %out_hbm.1, ...), custom_call_target="tpu_custom_call" | custom-call | tf_op jit(solution)/shard_map/pallas_call | solution.py:1005
  98.4 1.7 %convert_element_type.3 = bf16[192,512]{1,0:T(8,128)(2,1)} convert(f32[192,512]{1,0:T(8,128)} %shard_map.127) | non-fusion elementwise | flops 98304 | bytes 589824 | tf_op jit(solution)/shard_map/convert_element_type | solution.py:1110
